TPU v7x, 128 devices: a whole 4x4x4 slice. The times are simulated.
128 devices in a mesh: sp: 16 (over z, x), tp: 8 (over y, core).
Axes of the slice: x: 4, y: 4, z: 4, core: 2. Of those that a mesh axis runs over, the one named last changes fastest.
Arguments:
- latent: bfloat16 [2, 8192, 2048], P(None, ('sp', 'tp')), may hold values from -6 to 6
- context: bfloat16 [2, 1024, 2048], P(None, 'sp'), may hold values from -6 to 6
- cond: bfloat16 [2, 2048], replicated, may hold values from -6 to 6
- ctx_cond: bfloat16 [2048], replicated, may hold values from -6 to 6
- w_shift: bfloat16 [2048, 2048], P('sp', 'tp'), may hold values from -0.125 to 0.125
- w_scale: bfloat16 [2048, 2048], P('sp', 'tp'), may hold values from -0.125 to 0.125
- w_gate: bfloat16 [2048, 2048], P('sp', 'tp'), may hold values from -0.125 to 0.125
- norm_gain: float32 [2048], replicated, may hold values from 0.1 to 1.9
- w_query: bfloat16 [2048, 2048], P(None, 'tp'), may hold values from -1.08275726 to 1.08275726
- w_key: bfloat16 [2048, 2048], P(None, 'tp'), may hold values from -0.090598056 to 0.090598056
- w_value: bfloat16 [2048, 2048], P(None, 'tp'), may hold values from -0.125 to 0.125
- w_out: bfloat16 [2048, 2048], P('tp'), may hold values from -1.5 to 1.5
- rel_bias: float32 [32, 15, 31], P('tp'), may hold values from -4 to 4
- ctx_bias: float32 [32], P('tp'), may hold values from -3.5 to -2
Outputs:
- mixed: bfloat16 [2, 8192, 2048], P(None, ('sp', 'tp'))
All inputs are finite; a program needn't handle non-finite values.
Results may differ from a plain program's by a relative error of at most 0.0154.
Values may be sent and summed in bfloat16 or wider, within the bound.
A program may use at most 128 MiB of HBM per device.

v0:
```python
import functools

import jax
import jax.numpy as jnp
from jax import lax
from jax.experimental import pallas as pl
from jax.experimental.pallas import tpu as pltpu
from jax.sharding import PartitionSpec as P

HEAD_DIM = 64
GRID_W = 64
WIN_ROWS = 8
WIN_COLS = 16


EPSILON = 1e-06


def extended(shard, sides, width):
    for axis, dim in sides:
        size, length = (lax.axis_size(axis), shard.shape[dim])
        up = [(i, (i + 1) % size) for i in range(size - 1)]
        down = [(j, i) for i, j in up]
        last = lax.slice_in_dim(shard, length - width, length, axis=dim)
        first = lax.slice_in_dim(shard, 0, width, axis=dim)
        before = lax.ppermute(last, axis, up)
        after = lax.ppermute(first, axis, down)
        shard = jnp.concatenate([before, shard, after], axis=dim)
    return shard


def silu_rows(values):
    return jax.nn.silu(values.astype(jnp.float32)).astype(jnp.bfloat16)


def modulate_rows(rows, gain, shift, scale):
    floats = rows.astype(jnp.float32)
    inverse = lax.rsqrt(jnp.mean(floats * floats, axis=-1, keepdims=True) + EPSILON)
    return (floats * inverse * gain * (1.0 + scale) + shift).astype(jnp.bfloat16)

LOG2E = 1.4426950408889634


def attention_kernel(bias_ref, far_ref, q_ref, k_ref, v_ref, ck_ref, cv_ref, out_ref, table):
    pair = pl.program_id(0)
    rows_dev = q_ref.shape[1]
    padded = k_ref.shape[1]
    span = 2 * WIN_COLS
    half = WIN_COLS // 2
    reach = WIN_ROWS // 2
    nq, nk = rows_dev * WIN_COLS, padded * span
    lanes = 2 * HEAD_DIM

    @pl.when(pl.program_id(1) == 0)
    def _():
        sp = lax.axis_index("sp")
        rows_all = rows_dev * lax.axis_size("sp")
        at = lax.broadcasted_iota(jnp.int32, (WIN_COLS, nk), 1)
        p = lax.broadcasted_iota(jnp.int32, (WIN_COLS, nk), 0)
        key_row = sp * rows_dev - reach + at // span
        k = at % span
        inner = (k - p >= 0) & (k - p < WIN_COLS)
        edge = (p < half) == (k < WIN_COLS)
        for r in range(rows_dev):
            row = sp * rows_dev + r
            first = jnp.clip(row - reach, 0, rows_all - WIN_ROWS)
            inside = (key_row >= first) & (key_row < first + WIN_ROWS)
            shift = span * (r + reach - WIN_ROWS + 1) - half + 1
            for h in range(2):
                line = jnp.broadcast_to(bias_ref[0, h : h + 1, :], (WIN_COLS, nk))
                line = pltpu.roll(line, shift % nk, 1, stride=1, stride_axis=0) * LOG2E
                at_rows = pl.ds(r * WIN_COLS, WIN_COLS)
                table[h, 0, at_rows, :] = jnp.where(inside & edge, line, -jnp.inf)
                table[h, 1, at_rows, :] = jnp.where(inside & inner, line, -jnp.inf)

    factor = HEAD_DIM ** (-0.5) * LOG2E
    ck = ck_ref[...].reshape(-1, lanes)
    ctx_count = ck.shape[0]
    cv = jnp.concatenate([cv_ref[...].reshape(-1, lanes), jnp.ones((ctx_count, lanes), jnp.bfloat16)], axis=1)
    ones = jnp.ones((nk, lanes), jnp.bfloat16)
    low = lax.broadcasted_iota(jnp.int32, (nq, lanes), 1) < HEAD_DIM
    contract = (((1,), (1,)), ((), ()))
    every = q_ref[0].astype(jnp.float32)
    outs = []
    for block in range(GRID_W // WIN_COLS):
        if block == 0:
            q = jnp.concatenate([every[:, GRID_W - half :], every[:, :half]], axis=1)
        else:
            q = every[:, WIN_COLS * block - half : WIN_COLS * (block + 1) - half]
        q = q.astype(jnp.bfloat16).reshape(nq, lanes)

        def keys(ref):
            if block == 0:
                got = jnp.concatenate([ref[0, :, GRID_W - WIN_COLS :, :], ref[0, :, :WIN_COLS, :]], 1)
            else:
                got = ref[0, :, WIN_COLS * (block - 1) : WIN_COLS * (block + 1), :]
            return got.reshape(nk, lanes)

        k = keys(k_ref)
        v = jnp.concatenate([keys(v_ref), ones], axis=1)
        halves = []
        for h in range(2):
            mine = low if h == 0 else jnp.logical_not(low)
            one = jnp.where(mine, q, jnp.zeros_like(q))
            near = lax.dot_general(one, k, contract, preferred_element_type=jnp.float32)
            near = near * factor + table[h, min(block, 1)]
            far = lax.dot_general(one, ck, contract, preferred_element_type=jnp.float32)
            far = far * factor + far_ref[2 * pair + h] * LOG2E
            top = jnp.maximum(
                jnp.max(near, axis=-1, keepdims=True), jnp.max(far, axis=-1, keepdims=True)
            )
            near = jnp.exp2(near - top).astype(jnp.bfloat16)
            far = jnp.exp2(far - top).astype(jnp.bfloat16)
            got = jnp.dot(near, v, preferred_element_type=jnp.float32) + jnp.dot(
                far, cv, preferred_element_type=jnp.float32
            )
            halves.append(got[:, :lanes] / got[:, lanes:])
        outs.append(jnp.where(low, halves[0], halves[1]).reshape(rows_dev, WIN_COLS, lanes))
    outs = [outs[0][:, half:]] + outs[1:] + [outs[0][:, :half]]
    out_ref[0] = jnp.concatenate(outs, axis=1).astype(jnp.bfloat16)


def attention(query, pair, ctx_pair, rel_bias, ctx_bias):
    samples, rows_dev, _, cols = query.shape
    padded, ctx_count = pair.shape[1], ctx_pair.shape[0] * ctx_pair.shape[2]
    heads = cols // HEAD_DIM
    lanes = 2 * HEAD_DIM
    pairs = cols // lanes
    nq, nk = rows_dev * WIN_COLS, padded * 2 * WIN_COLS
    flat = jnp.pad(rel_bias, ((0, 0), (0, 1), (0, 1))).reshape(heads, -1)
    flat = jnp.pad(flat, ((0, 0), (0, nk - flat.shape[1]))).reshape(pairs, 2, nk)
    token = lambda at: pl.BlockSpec((1, padded, GRID_W, lanes), lambda p, s: (s, 0, 0, p + at))
    far = lambda at: pl.BlockSpec(
        (ctx_pair.shape[0], 1, ctx_pair.shape[2], lanes), lambda p, s: (0, s, 0, p + at)
    )
    own = pl.BlockSpec((1, rows_dev, GRID_W, lanes), lambda p, s: (s, 0, 0, p))
    scores = samples * heads * 4 * nq * (nk + ctx_count)
    return pl.pallas_call(
        attention_kernel,
        grid=(pairs, samples),
        out_shape=jax.ShapeDtypeStruct(query.shape, jnp.bfloat16),
        in_specs=[
            pl.BlockSpec((1, 2, nk), lambda p, s: (p, 0, 0)),
            pl.BlockSpec(memory_space=pltpu.SMEM),
            own,
            token(0),
            token(pairs),
            far(0),
            far(pairs),
        ],
        out_specs=own,
        scratch_shapes=[pltpu.VMEM((2, 2, nq, nk), jnp.float32)],
        cost_estimate=pl.CostEstimate(
            flops=scores * 512, bytes_accessed=8 * query.size * 2, transcendentals=scores
        ),
    )(flat, ctx_bias, query, pair, pair, ctx_pair, ctx_pair)


def on_device(
    latent,
    context,
    cond,
    ctx_cond,
    w_shift,
    w_scale,
    w_gate,
    norm_gain,
    w_query,
    w_key,
    w_value,
    w_out,
    rel_bias,
    ctx_bias,
):
    samples = latent.shape[0]
    rows_sp = w_shift.shape[0]
    local_cols = w_shift.shape[1]
    sp_index = lax.axis_index("sp")
    ada = silu_rows(jnp.concatenate([cond, ctx_cond[None, :]], axis=0))
    ada_rows = lax.dynamic_slice_in_dim(ada, sp_index * rows_sp, rows_sp, 1)
    partial_value = jnp.stack(
        [
            jnp.dot(ada_rows, weight, preferred_element_type=jnp.float32)
            for weight in (w_shift, w_scale, w_gate)
        ]
    )
    summed = lax.psum(partial_value, "sp")
    modulation = lax.all_gather(summed, "tp", axis=2, tiled=True)
    hidden = modulate_rows(
        latent, norm_gain, modulation[0, :samples, None, :], modulation[1, :samples, None, :]
    )
    w_triple = jnp.concatenate([w_query, w_key, w_value], axis=1)
    triple = jnp.dot(
        lax.all_gather(hidden, "tp", axis=1, tiled=True),
        w_triple,
        preferred_element_type=jnp.float32,
    ).astype(jnp.bfloat16)
    ctx_hidden = modulate_rows(context, norm_gain, modulation[0, samples], modulation[1, samples])
    w_pair = jnp.concatenate([w_key, w_value], axis=1)
    own_pair = jnp.dot(ctx_hidden, w_pair, preferred_element_type=jnp.float32).astype(jnp.bfloat16)
    ctx_pair = lax.all_gather(own_pair, "sp", axis=1, tiled=True)
    heads = local_cols // HEAD_DIM
    tokens_sp = triple.shape[1]
    rows_dev = tokens_sp // GRID_W
    rows_all = rows_dev * lax.axis_size("sp")
    reach = WIN_ROWS // 2
    query = triple[..., :local_cols].reshape(samples, rows_dev, GRID_W, local_cols)
    pair = triple[..., local_cols:].reshape(samples, rows_dev, GRID_W, 2 * local_cols)
    padded_pair = extended(pair, (("sp", 1),), reach)
    mixed = attention(query, padded_pair, ctx_pair[None], rel_bias, ctx_bias)
    attended = mixed.reshape(samples, tokens_sp, local_cols)
    attended = attended.transpose(1, 0, 2)
    update = lax.psum_scatter(
        jnp.einsum("tsc,cd->tsd", attended, w_out, preferred_element_type=jnp.float32).astype(
            jnp.bfloat16
        ),
        "tp",
        scatter_dimension=0,
        tiled=True,
    ).astype(jnp.float32)
    gate = modulation[2, :samples, None, :]
    result = latent.astype(jnp.float32) + gate * update.transpose(1, 0, 2)
    return result.astype(jnp.bfloat16)


MESH = pl.DeviceIdType.MESH


def entry_barrier(peers):
    barrier = pltpu.get_barrier_semaphore()
    for device, there in peers:
        @pl.when(there)
        def _():
            pl.semaphore_signal(barrier, inc=1, device_id=device, device_id_type=MESH)
    pl.semaphore_wait(barrier, sum(jnp.where(there, 1, 0) for _, there in peers))


def front_kernel(
    ada_ref, ws_ref, wc_ref, wg_ref, gain_ref, latent_ref, ctx_ref, wq_ref, wk_ref, wv_ref,
    full_ref, q_ref, kv_ref, ckv_ref,
    part, got, total, full, buf, wq, wkv, own_sem, s1, r1, s2, r2, s_ext, r_ext, s_ctx, r_ctx, r_sib,
):
    sp, tp = lax.axis_index("sp"), lax.axis_index("tp")
    n_sp, n_tp = lax.axis_size("sp"), lax.axis_size("tp")
    cols = part.shape[1]
    over_sp = [lax.rem(sp + k, n_sp) for k in range(1, n_sp)]
    over_tp = [lax.rem(tp + k, n_tp) for k in range(1, n_tp)]
    always = sp >= 0
    y, c = tp // 2, lax.rem(tp, 2)
    z, x = sp // 2, lax.rem(sp, 2)
    n_z = n_sp // 2
    sib, across = y * 2 + 1 - c, (1 - y) * 2 + c
    has_up, has_down = sp > 0, sp < n_sp - 1
    direct = y * c + (1 - y) * (6 + c)
    indirect = (1 - y) * c + y * (6 + c)
    has_direct = ((y == 1) & has_up) | ((y == 0) & has_down)
    has_indirect = ((y == 0) & has_up) | ((y == 1) & has_down)
    toward = sp + 2 * y - 1
    here, there = (sp, sib), (sp, across)
    own_slot, across_slot = 2 + tp, 2 + across
    x_peer = sp + 1 - 2 * x
    beside, up, down = (x_peer, tp), (sp + 2, tp), (sp - 2, tp)
    can_up, can_down = sp + 2 < n_sp, sp >= 2
    half = buf.shape[1] // 2
    part_of = pl.ds(pl.multiple_of(c * half, half), half)

    locals_ = [
        pltpu.make_async_copy(wq_ref, wq, own_sem.at[0]),
        pltpu.make_async_copy(wk_ref, wkv.at[:, pl.ds(0, cols)], own_sem.at[1]),
        pltpu.make_async_copy(wv_ref, wkv.at[:, pl.ds(cols, cols)], own_sem.at[2]),
    ]
    for copy in locals_:
        copy.start()
    own_copies = [
        pltpu.make_async_copy(latent_ref.at[s], buf.at[2 * own_slot + s], own_sem.at[3 + s])
        for s in range(2)
    ] + [
        pltpu.make_async_copy(ctx_ref.at[s], buf.at[16 + sp, pl.ds(half * s, half)], own_sem.at[5 + s])
        for s in range(2)
    ]
    for copy in own_copies:
        copy.start()
    entry_barrier([((p, tp), always) for p in over_sp] + [((sp, p), always) for p in over_tp])

    early = []
    mode = ["start"]

    def send(cond, copy):
        @pl.when(cond)
        def _():
            if mode[0] == "start":
                copy.start()
            else:
                copy.wait_send()

    def begin(cond, copy):
        early.append((cond, copy))
        send(cond, copy)

    def arrived(cond, copy):
        if mode[0] == "start":
            @pl.when(cond)
            def _():
                copy.wait_recv()

    def piece(flow, s, device, slot, own=False):
        return pltpu.make_async_remote_copy(
            src_ref=latent_ref.at[s] if own else buf.at[2 * slot + s],
            dst_ref=buf.at[2 * slot + s],
            send_sem=s_ext.at[flow, s], recv_sem=r_ext.at[flow, s],
            device_id=device, device_id_type=MESH,
        )

    def block(at, way, device, own=False):
        return pltpu.make_async_remote_copy(
            src_ref=ctx_ref.at[c] if own else buf.at[16 + at, part_of],
            dst_ref=buf.at[16 + at, part_of],
            send_sem=s_ctx.at[at, way], recv_sem=(r_sib if way == 3 else r_ctx).at[at],
            device_id=device, device_id_type=MESH,
        )

    def first(k, peer):
        return pltpu.make_async_remote_copy(
            src_ref=part, dst_ref=got.at[k], send_sem=s1.at[k], recv_sem=r1.at[k],
            device_id=(peer, tp), device_id_type=MESH,
        )

    columns = pl.ds(pl.multiple_of(tp * cols, cols), cols)

    def second(k, peer):
        return pltpu.make_async_remote_copy(
            src_ref=total, dst_ref=full.at[:, columns], send_sem=s2.at[k], recv_sem=r2.at[k],
            device_id=(sp, peer), device_id_type=MESH,
        )

    for at, weight in enumerate((ws_ref, wc_ref, wg_ref)):
        value = jnp.dot(ada_ref[...], weight[...], preferred_element_type=jnp.float32)
        part[8 * at : 8 * at + 8, :] = value[:8]
    firsts = [first(k, peer) for k, peer in enumerate(over_sp)]
    for copy in firsts:
        copy.start()
    begin(always, piece(1, 0, there, own_slot, True))
    begin(always, block(sp, 0, beside, True))
    begin(can_up, block(sp, 1, up, True))
    begin(can_down, block(sp, 2, down, True))
    for s in range(2):
        begin(has_indirect, piece(2, s, (toward, tp), direct, True))
    for s in range(2):
        begin(always, piece(0, s, here, own_slot, True))
    value = part[...]
    for k, copy in enumerate(firsts):
        copy.wait()
        value = value + got[k]
    total[...] = value
    seconds = [second(k, peer) for k, peer in enumerate(over_tp)]
    for copy in seconds:
        copy.start()
    begin(always, piece(1, 1, there, own_slot, True))
    full[:, columns] = value
    for copy in locals_ + own_copies:
        copy.wait()
    for copy in seconds:
        copy.wait()
    full_ref[...] = full[...]

    def neighbour_block():
        arrived(always, block(x_peer, 0, beside))
        send((c == 0) & can_up, block(x_peer, 1, up))
        send((c == 0) & can_down, block(x_peer, 2, down))
        send(always, block(x_peer, 3, here))

    def relay(hop):
        for e in range(2):
            straight = (c == 0) | (x == e)
            crossing = (c == 1) & (x == e)
            low, high = sp - x - 2 * hop + e, sp - x + 2 * hop + e
            for at, way, device, can, there_is in (
                (lax.max(low, 0), 1, up, can_up, low >= 0),
                (lax.min(high, n_sp - 1), 2, down, can_down, high < n_sp),
            ):
                arrived(there_is, block(at, way, device))
                send(there_is & can & straight, block(at, way, device))
                send(there_is & crossing, block(at, 0, beside))
                send(there_is, block(at, 3, here))

    def from_across(s):
        arrived(always, piece(1, s, there, across_slot))
        send(always, piece(3, s, here, across_slot))

    def from_direct(s):
        arrived(has_direct, piece(2, s, here, direct))
        send(has_direct, piece(5, s, there, direct))
        send(has_direct, piece(6, s, here, direct))

    def from_indirect(s):
        arrived(has_indirect, piece(5, s, there, indirect))
        send(has_indirect, piece(7, s, here, indirect))

    def sibling(flow, s, cond=always):
        arrived(cond, piece(flow, s, here, own_slot))

    def far_block(h, e):
        zb = lax.rem(z + h, n_z)
        at = 2 * zb + e
        arrived(always, block(at, 3, here))

    plan = []

    def add(kind, s, events, at=0):
        plan.append((kind, s, events, at))

    both = lambda flow, cond=always: [functools.partial(sibling, flow, e, cond) for e in range(2)]
    add(0, 0, [])
    add(1, 0, [neighbour_block] + both(0))
    from_peer = lambda: arrived(always, block(x_peer, 3, here))
    add(8, 0, [functools.partial(from_across, 0), functools.partial(from_direct, 0), from_peer], 2 * z)
    add(2, 0, [functools.partial(relay, 1), functools.partial(from_across, 1)])
    add(4, 0, [functools.partial(from_direct, 1)])
    add(3, 0, [functools.partial(relay, 2)] + both(3))
    add(5, 0, both(6, has_direct))
    hops = [functools.partial(relay, hop) for hop in range(3, n_z)]
    for h in range(1, n_z):
        waits = [functools.partial(far_block, h, e) for e in range(2)]
        add(8, 0, (hops + [functools.partial(from_indirect, 0)] if h == 1 else []) + waits, 2 * lax.rem(z + h, n_z))
    add(6, 0, [functools.partial(from_indirect, 1)])
    add(7, 0, both(7, has_indirect))

    slots = (own_slot, 2 + sib, across_slot, 2 + (1 - y) * 2 + 1 - c,
             direct, direct + 1 - 2 * c, indirect, indirect + 1 - 2 * c)

    def step(i, carry):
        at = 0
        row = 0
        exists = 0
        wants = 0
        for k, (kind, s, events, ctx_at) in enumerate(plan):
            on = jnp.where(i == k, 1, 0)
            at = at + on * (16 + ctx_at if kind == 8 else 2 * slots[kind])
            row = row + on * (1 if kind == 8 else 0)
            there_is = has_direct if kind in (4, 5) else has_indirect if kind in (6, 7) else always
            exists = exists + on * jnp.where(there_is, 1, 0)
            wants = wants + on * (1 if kind < 4 else 0)
            if events:
                @pl.when(i == k)
                def _():
                    for event in events:
                        event()

        @pl.when(exists == 1)
        def _():
            hidden = []
            for e in range(2):
                rows = buf[at + e].astype(jnp.float32)
                inverse = lax.rsqrt(jnp.mean(rows * rows, axis=-1, keepdims=True) + EPSILON)
                which = e + row * (2 - e)
                lift = gain_ref[...] * (1.0 + full[pl.ds(8 + which, 1), :])
                rows = rows * inverse * lift + full[pl.ds(which, 1), :]
                hidden.append(rows.astype(jnp.bfloat16))
            hidden = jnp.concatenate(hidden, axis=0)
            count = hidden.shape[0] // 2
            pair = jnp.dot(hidden, wkv[...], preferred_element_type=jnp.float32).astype(jnp.bfloat16)

            @pl.when(at < 16)
            def _():
                for e in range(2):
                    kv_ref[lax.div(lax.min(at, 14), 2) + 8 * e] = pair[e * count : (e + 1) * count]

            @pl.when(at >= 16)
            def _():
                for e in range(2):
                    ckv_ref[lax.max(at - 16, 0) + e] = pair[e * count : (e + 1) * count]

            @pl.when(wants == 1)
            def _():
                query = jnp.dot(hidden, wq[...], preferred_element_type=jnp.float32)
                query = query.astype(jnp.bfloat16)
                for e in range(2):
                    place = lax.div(lax.min(lax.max(at - 4, 0), 6), 2) + 4 * e
                    q_ref[place] = query[e * count : (e + 1) * count]

        @pl.when(exists == 0)
        def _():
            for e in range(2):
                kv_ref[lax.div(lax.min(at, 14), 2) + 8 * e] = jnp.zeros(kv_ref.shape[1:], jnp.bfloat16)

        return carry

    lax.fori_loop(0, len(plan), step, 0)
    mode[0] = "drain"
    for cond, copy in early:
        send(cond, copy)
    for _, _, events, _ in plan:
        for event in events:
            event()


def front(ada_rows, mods, gain, latent, context, w_query, w_key, w_value):
    n_sp, n_tp = lax.axis_size("sp"), lax.axis_size("tp")
    samples, tokens, width = latent.shape
    cols = w_query.shape[1]
    block = (24, cols)
    ada_rows = jnp.pad(ada_rows, ((0, 16 - ada_rows.shape[0]), (0, 0)))
    vmem, hbm = pl.BlockSpec(memory_space=pltpu.VMEM), pl.BlockSpec(memory_space=pl.ANY)
    dma = pltpu.SemaphoreType.DMA
    return pl.pallas_call(
        front_kernel,
        out_shape=(
            jax.ShapeDtypeStruct((24, width), jnp.float32),
            jax.ShapeDtypeStruct((samples * n_tp, tokens, cols), jnp.bfloat16),
            jax.ShapeDtypeStruct((samples * 8, tokens, 2 * cols), jnp.bfloat16),
            jax.ShapeDtypeStruct((n_sp, samples * context.shape[1], 2 * cols), jnp.bfloat16),
        ),
        in_specs=[vmem] * 7 + [hbm] * 3,
        out_specs=[vmem] * 4,
        scratch_shapes=[
            pltpu.VMEM(block, jnp.float32),
            pltpu.VMEM((n_sp - 1,) + block, jnp.float32),
            pltpu.VMEM(block, jnp.float32),
            pltpu.VMEM((24, width), jnp.float32),
            pltpu.VMEM((16 + n_sp, tokens, width), jnp.bfloat16),
            pltpu.VMEM((width, cols), jnp.bfloat16),
            pltpu.VMEM((width, 2 * cols), jnp.bfloat16),
            dma((7,)), dma((n_sp - 1,)), dma((n_sp - 1,)), dma((n_tp - 1,)), dma((n_tp - 1,)),
            dma((8, 2)), dma((8, 2)), dma((n_sp, 4)), dma((n_sp,)), dma((n_sp,)),
        ],
        compiler_params=pltpu.CompilerParams(
            collective_id=1, has_side_effects=True, vmem_limit_bytes=60 * 2**20
        ),
    )(ada_rows, *mods, gain[None, :], latent, context, w_query, w_key, w_value)


def scatter_kernel(parts_ref, out_ref, got, summed, far, s1, r1, s2, r2):
    sp, tp = lax.axis_index("sp"), lax.axis_index("tp")
    y, c = tp // 2, lax.rem(tp, 2)
    sib, across = y * 2 + 1 - c, (1 - y) * 2 + c
    sib_across = (1 - y) * 2 + 1 - c
    entry_barrier([((sp, sib), sp >= 0), ((sp, across), sp >= 0)])
    chunks = far.shape[0]
    rows = far.shape[1]

    def near(k):
        at = k % chunks
        target = sib_across if k < chunks else sib
        return pltpu.make_async_remote_copy(
            src_ref=parts_ref.at[target, pl.ds(at * rows, rows)],
            dst_ref=got.at[k],
            send_sem=s1.at[k], recv_sem=r1.at[k],
            device_id=(sp, sib), device_id_type=MESH,
        )

    def cross(k):
        return pltpu.make_async_remote_copy(
            src_ref=summed.at[k],
            dst_ref=far.at[k],
            send_sem=s2.at[k], recv_sem=r2.at[k],
            device_id=(sp, across), device_id_type=MESH,
        )

    for k in range(2 * chunks):
        near(k).start()
    for k in range(chunks):
        near(k).wait()
        mine = parts_ref[across, k * rows : (k + 1) * rows, :].astype(jnp.float32)
        summed[k] = (mine + got[k].astype(jnp.float32)).astype(jnp.bfloat16)
        cross(k).start()
    for k in range(chunks):
        near(chunks + k).wait()
        cross(k).wait()
        mine = parts_ref[tp, k * rows : (k + 1) * rows, :].astype(jnp.float32)
        mine = mine + got[chunks + k].astype(jnp.float32) + far[k].astype(jnp.float32)
        out_ref[k * rows : (k + 1) * rows, :] = mine


def scatter_sum(parts):
    _, tokens, width = parts.shape
    chunks = 4
    rows = tokens // chunks
    sems = [pltpu.SemaphoreType.DMA((2 * chunks,))] * 2 + [pltpu.SemaphoreType.DMA((chunks,))] * 2
    return pl.pallas_call(
        scatter_kernel,
        out_shape=jax.ShapeDtypeStruct((tokens, width), jnp.float32),
        in_specs=[pl.BlockSpec(memory_space=pltpu.VMEM)],
        out_specs=pl.BlockSpec(memory_space=pltpu.VMEM),
        scratch_shapes=[
            pltpu.VMEM((2 * chunks, rows, width), jnp.bfloat16),
            pltpu.VMEM((chunks, rows, width), jnp.bfloat16),
            pltpu.VMEM((chunks, rows, width), jnp.bfloat16),
        ]
        + sems,
        compiler_params=pltpu.CompilerParams(
            collective_id=3, has_side_effects=True, vmem_limit_bytes=40 * 2**20
        ),
    )(parts)


def on_four(
    latent, context, cond, ctx_cond, w_shift, w_scale, w_gate, norm_gain,
    w_query, w_key, w_value, w_out, rel_bias, ctx_bias,
):
    samples, tokens, width = latent.shape
    n_sp, n_tp = lax.axis_size("sp"), lax.axis_size("tp")
    rows_sp, local_cols = w_shift.shape
    sp = lax.axis_index("sp")
    ada = silu_rows(jnp.concatenate([cond, ctx_cond[None, :]], axis=0))
    ada_rows = lax.dynamic_slice_in_dim(ada, sp * rows_sp, rows_sp, 1)
    modulation, query, pair, ctx_pair = front(
        ada_rows, (w_shift, w_scale, w_gate), norm_gain, latent, context, w_query, w_key, w_value
    )
    modulation = modulation.reshape(3, 8, width)
    rows_dev = n_tp * tokens // GRID_W
    query = query.reshape(samples, rows_dev, GRID_W, local_cols)
    pair = pair.reshape(samples, 2 * rows_dev, GRID_W, 2 * local_cols)
    ctx_pair = ctx_pair.reshape(n_sp, samples, -1, 2 * local_cols)
    mixed = attention(query, pair, ctx_pair, rel_bias, ctx_bias)
    attended = mixed.reshape(samples, n_tp, tokens, local_cols)
    attended = attended.transpose(1, 0, 2, 3).reshape(n_tp, samples * tokens, local_cols)
    parts = jnp.dot(attended, w_out, preferred_element_type=jnp.float32).astype(jnp.bfloat16)
    update = scatter_sum(parts).reshape(samples, tokens, width)
    gate = modulation[2, :samples, None, :]
    return (latent.astype(jnp.float32) + gate * update).astype(jnp.bfloat16)


def solution(mesh):
    shape = dict(mesh.shape)
    quick = shape["tp"] == 4 and shape["sp"] == 8
    return jax.shard_map(
        on_four if quick else on_device,
        mesh=mesh,
        in_specs=(
            P(None, ("sp", "tp"), None),
            P(None, "sp", None),
            P(),
            P(),
            P("sp", "tp"),
            P("sp", "tp"),
            P("sp", "tp"),
            P(),
            P(None, "tp"),
            P(None, "tp"),
            P(None, "tp"),
            P("tp", None),
            P("tp", None, None),
            P("tp"),
        ),
        out_specs=P(None, ("sp", "tp"), None),
        check_vma=False,
    )
```

profile of v0, /device:TPU:1, one launch (start us, length us, event | category | flops | bytes accessed | tf_op | source)
XLA Modules:
  0.0 243.6 jit_solution(8858065226888468013)
XLA Ops:
  6.6 0.8 broadcast_in_dim.4
  8.2 1.0 convolution_bitcast_fusion
  9.1 1.0 convolution_bitcast_fusion.1
  10.1 1.0 convolution_bitcast_fusion.2
  11.1 62.2 %psum.7 = f32[3,3,256]{2,1,0:T(4,128)S(1)} all-reduce(f32[3,3,256]{2,1,0:T(4,128)S(1)} %pad_maximum_fusion.1), channel_id=1, replica_groups=mesh['sp'=16,'tp'=8] {'sp'}, use_global_device_ids=true, to_apply=%region_0.1 | all-reduce | flops 2304 | bytes 18432 | tf_op jit(solution)/shard_map/psum | solution.py:187
  73.3 28.0 %all_gather.9 = f32[3,3,2048]{2,1,0:T(4,128)S(1)} all-gather(f32[3,3,256]{2,1,0:T(4,128)S(1)} %psum.7), channel_id=1, replica_groups=mesh['sp'=16,'tp'=8] {'tp'}, dimensions={2}, use_global_device_ids=true | all-gather | bytes 82944 | tf_op jit(solution)/shard_map/all_gather | solution.py:188
  101.3 1.2 fusion.15
  102.5 2.1 fusion.19
  104.8 1.2 fusion.10
  106.1 2.4 fusion.9
  108.5 24.0 %all-gather.3.cloned.1.call-done = bf16[2,512,2048]{2,1,0:T(8,128)(2,1)} async-done(((bf16[2,64,2048]{2,1,0:T(8,128)(2,1)}), bf16[2,512,2048]{2,1,0:T(8,128)(2,1)}) %all-gather.3.cloned.1.call-update) | async-done | bytes 4194320 | tf_op jit(solution)/shard_map/all_gather | solution.py:194
  132.6 6.2 %fusion.8 = bf16[2,512,768]{2,1,0:T(8,128)(2,1)S(1)} fusion(bf16[2,512,2048]{2,1,0:T(8,128)(2,1)} %all-gather.3.cloned.1.call-done, bf16[2048,256]{1,0:T(8,128)(2,1)S(1)} %copy-done.6, bf16[2048,256]{1,0:T(8,128)(2,1)} %param.23, bf16[2048,256]{1,0:T(8,128)(2,1)} %param.22), kind=kOutput, calls=%fused_computation.12 | convolution fusion | flops 3231449088 | bytes 8912896 | tf_op jit(solution)/shard_map/dot_general | solution.py:193
  138.8 1.1 copy-done.2
  140.1 3.9 %collective-permute-start = (bf16[2,4,64,512]{3,2,1,0:T(8,128)(2,1)S(1)}, bf16[2,4,64,512]{3,2,1,0:T(8,128)(2,1)}, u32[]{:S(2)}, u32[]{:S(2)}) collective-permute-start(bf16[2,4,64,512]{3,2,1,0:T(8,128)(2,1)S(1)} %get-tuple-element.5), channel_id=1, source_target_pairs={{0,8},{8,16},{16,24},{24,32},{32,40},{40,48},{48,56},{56,64},{64,7... | collective-permute-start | bytes 1572872 | tf_op jit(solution)/shard_map/ppermute | solution.py:26
  144.0 1.3 collective-permute-start.1
  146.0 1.9 slice.39
  147.9 8.4 %collective-permute-done = bf16[2,4,64,512]{3,2,1,0:T(8,128)(2,1)} collective-permute-done((bf16[2,4,64,512]{3,2,1,0:T(8,128)(2,1)S(1)}, bf16[2,4,64,512]{3,2,1,0:T(8,128)(2,1)}, u32[]{:S(2)}, u32[]{:S(2)}) %collective-permute-start) | collective-permute-done | bytes 524320 | tf_op jit(solution)/shard_map/ppermute | solution.py:26
  156.3 4.0 %collective-permute-done.1 = bf16[2,4,64,512]{3,2,1,0:T(8,128)(2,1)} collective-permute-done((bf16[2,4,64,512]{3,2,1,0:T(8,128)(2,1)S(1)}, bf16[2,4,64,512]{3,2,1,0:T(8,128)(2,1)}, u32[]{:S(2)}, u32[]{:S(2)}) %collective-permute-start.1) | collective-permute-done | bytes 524320 | tf_op jit(solution)/shard_map/ppermute | solution.py:27
  160.3 2.8 %pad_maximum_fusion.k_ref.v_ref = bf16[2,16,64,512]{3,2,1,0:T(8,128)(2,1)} fusion(bf16[2,4,64,512]{3,2,1,0:T(8,128)(2,1)} %collective-permute-done.1, bf16[2,8,64,512]{3,2,1,0:T(8,128)(2,1)S(1)} %bitcast.41, bf16[2,4,64,512]{3,2,1,0:T(8,128)(2,1)} %collective-permute-done), kind=kLoop, calls=%fused_computation.7 | loop fusion | flops 2097152 | bytes 4194304 | tf_op jit(solution)/shard_map/concatenate | solution.py:28
  163.1 19.4 %all-gather.5.cloned.1.call-done = bf16[2,1024,512]{2,1,0:T(8,128)(2,1)} async-done(((bf16[2,64,512]{2,1,0:T(8,128)(2,1)}), bf16[2,1024,512]{2,1,0:T(8,128)(2,1)}) %all-gather.5.cloned.1.call-update) | async-done | bytes 2097168 | tf_op jit(solution)/shard_map/all_gather | solution.py:201
  182.5 12.2 %shard_map.136 = bf16[2,8,64,256]{3,2,1,0:T(8,128)(2,1)} custom-call(f32[2,2,512]{2,1,0:T(2,128)} %reshape.42.bias_ref, f32[4]{0:T(128)} %far_ref.1, bf16[2,8,64,256]{3,2,1,0:T(8,128)(2,1)} %bitcast.42, bf16[2,16,64,512]{3,2,1,0:T(8,128)(2,1)} %pad_maximum_fusion.k_ref.v_ref, bf16[2,16,64,512]{3,2,1,0:T(8,128)(2,1)} %pad_maximum_fusion.k_ref.v_ref, ...), custom_call_target="tpu_custom_call" | custom-call | flops 3221225472 | bytes 4194304 | tf_op jit(solution)/shard_map/pallas_call | solution.py:138
  194.7 4.2 %convolution_convert_fusion = bf16[512,2,2048]{2,0,1:T(8,128)(2,1)} fusion(bf16[512,2,256]{2,0,1:T(8,128)(2,1)} %bitcast.43, bf16[256,2048]{1,0:T(8,128)(2,1)S(1)} %copy-done), kind=kOutput, calls=%fused_computation | convolution fusion | flops 1075838976 | bytes 5767168 | tf_op jit(solution)/shard_map/tsc,cd->tsd/dot_general | solution.py:214
  199.0 36.0 %reduce-scatter.2.cloned.1.call-done = bf16[64,2,2048]{2,0,1:T(8,128)(2,1)} async-done(((bf16[512,2,2048]{2,0,1:T(8,128)(2,1)}), bf16[64,2,2048]{2,0,1:T(8,128)(2,1)}) %reduce-scatter.2.cloned.1.call-update) | async-done | bytes 524304 | tf_op jit(solution)/shard_map/reduce_scatter | solution.py:213
  235.1 2.0 fusion.20
  (30 shorter events, 1.8 us)
Async XLA Ops:
  6.5 188.2 %copy-start = (bf16[256,2048]{1,0:T(8,128)(2,1)S(1)}, bf16[256,2048]{1,0:T(8,128)(2,1)}, u32[]{:S(2)}) copy-start(bf16[256,2048]{1,0:T(8,128)(2,1)} %param.25) | copy-start | bytes 3145732
  6.5 99.5 %copy-start.5 = (f32[2048]{0:T(1024)S(1)}, f32[2048]{0:T(1024)}, u32[]{:S(2)}) copy-start(f32[2048]{0:T(1024)} %param.21) | copy-start | bytes 24580
  6.5 99.5 %copy-start.3 = (bf16[2,64,2048]{2,1,0:T(8,128)(2,1)S(1)}, bf16[2,64,2048]{2,1,0:T(8,128)(2,1)}, u32[]{:S(2)}) copy-start(bf16[2,64,2048]{2,1,0:T(8,128)(2,1)} %param.15) | copy-start | bytes 1572868
  6.5 99.5 %copy-start.6 = (bf16[2048,256]{1,0:T(8,128)(2,1)S(1)}, bf16[2048,256]{1,0:T(8,128)(2,1)}, u32[]{:S(2)}) copy-start(bf16[2048,256]{1,0:T(8,128)(2,1)} %param.24) | copy-start | bytes 3145732
  6.5 126.0 %all-gather.3.cloned.1.call-start = ((), (), s32[]{:S(2)}) async-start(), calls=%async_computation.1 | async-start | bytes 4718592 | tf_op jit(solution)/shard_map/all_gather | solution.py:194
  104.7 77.8 %all-gather.5.cloned.1.call-start = ((), (), s32[]{:S(2)}) async-start(), calls=%async_computation.2 | async-start | bytes 2228224 | tf_op jit(solution)/shard_map/all_gather | solution.py:201
  108.5 126.6 %reduce-scatter.2.cloned.1.call-start = ((), (), s32[]{:S(2)}) async-start(), calls=%async_computation.3 | async-start | bytes 4718592 | tf_op jit(solution)/shard_map/reduce_scatter | solution.py:213
  138.8 1.1 copy-start.2
  139.9 5.4 %copy-start.4 = (f32[4,15,31]{2,0,1:T(4,128)S(1)}, f32[4,15,31]{2,0,1:T(4,128)}, u32[]{:S(2)}) copy-start(f32[4,15,31]{2,0,1:T(4,128)} %param.26) | copy-start | bytes 22324
  140.1 16.2 %collective-permute-start = (bf16[2,4,64,512]{3,2,1,0:T(8,128)(2,1)S(1)}, bf16[2,4,64,512]{3,2,1,0:T(8,128)(2,1)}, u32[]{:S(2)}, u32[]{:S(2)}) collective-permute-start(bf16[2,4,64,512]{3,2,1,0:T(8,128)(2,1)S(1)} %get-tuple-element.5), channel_id=1, source_target_pairs={{0,8},{8,16},{16,24},{24,32},{32,40},{40,48},{48,56},{56,64},{64,7... | collective-permute-start | bytes 1572872 | tf_op jit(solution)/shard_map/ppermute | solution.py:26
  144.0 16.3 %collective-permute-start.1 = (bf16[2,4,64,512]{3,2,1,0:T(8,128)(2,1)S(1)}, bf16[2,4,64,512]{3,2,1,0:T(8,128)(2,1)}, u32[]{:S(2)}, u32[]{:S(2)}) collective-permute-start(bf16[2,4,64,512]{3,2,1,0:T(8,128)(2,1)S(1)} %get-tuple-element.6), channel_id=1, source_target_pairs={{8,0},{16,8},{24,16},{32,24},{40,32},{48,40},{56,48},{64,56},{72,6... | collective-permute-start | bytes 1572872 | tf_op jit(solution)/shard_map/ppermute | solution.py:27
  199.0 36.1 %copy-start.1 = (bf16[2,64,2048]{2,1,0:T(8,128)(2,1)S(1)}, bf16[2,64,2048]{2,1,0:T(8,128)(2,1)}, u32[]{:S(2)}) copy-start(bf16[2,64,2048]{2,1,0:T(8,128)(2,1)} %param.14) | copy-start | bytes 1572868
Sparse Core Ops, SparseCore 0:
  104.8 27.6 all-gather.2
  134.7 47.7 all-gather.4
  199.1 35.8 reduce-scatter.1
where the time goes:
time: 247 us; the launch traced here: 244 us
  waiting for transfers between devices  92 us (37%)
  blocking collectives  90.2 us (37%)
  matrix products  15.8 us (6%)
  between operations  13.2 us (5%)
  Pallas kernels  12.2 us (5%)
  other arithmetic  10.1 us (4%)
  starting transfers between devices  5.3 us (2%)
  local copies, waits for them, and re-layouts  4.74 us (2%)
    psum x1, blocking collectives, on_device(): summed = lax.psum(partial_value, 'sp')  62.2 us
    reduce_scatter x1, waiting for transfers between devices, on_device(): lax.psum_scatter(jnp.einsum('tsc,cd->tsd', attended, w_out, preferred_ele...  36 us
    all_gather x1, blocking collectives, on_device(): modulation = lax.all_gather(summed, 'tp', axis=2, tiled=True)  28 us
    all_gather x1, waiting for transfers between devices, on_device(): lax.all_gather(hidden, 'tp', axis=1, tiled=True)  24 us
    all_gather x1, waiting for transfers between devices, on_device(): ctx_pair = lax.all_gather(own_pair, 'sp', axis=1, tiled=True)  19.4 us
    pallas_call x1, Pallas kernels, attention(): pl.pallas_call(attention_kernel, grid=(pairs, samples), out_shape=jax.Sha...  12.2 us
    ppermute x1, waiting for transfers between devices, extended(): before = lax.ppermute(last, axis, up)  8.41 us
    dot_general x1, matrix products, on_device(): jnp.dot(lax.all_gather(hidden, 'tp', axis=1, tiled=True), w_triple, prefe...  6.2 us
  transfers between devices with their start and end apart: 5, of which 5 were waited for; matrix products, arithmetic and copies ran while one was open for 6% of the time, Pallas kernels for 0%

commit v1 on v0

v1 whole, which is shorter than its diff:
```python
import functools

import jax
import jax.numpy as jnp
from jax import lax
from jax.experimental import pallas as pl
from jax.experimental.pallas import tpu as pltpu
from jax.sharding import PartitionSpec as P

HEAD_DIM = 64
GRID_W = 64
WIN_ROWS = 8
WIN_COLS = 16
EPSILON = 1e-06
LOG2E = 1.4426950408889634
MESH = pl.DeviceIdType.MESH

N_X, N_Z, N_Y = 4, 4, 4
PAD_ROWS = 16
KEY_ROWS = 10
REACH = WIN_ROWS // 2


def remote(src, dst, send, recv, device):
    return pltpu.make_async_remote_copy(
        src_ref=src, dst_ref=dst, send_sem=send, recv_sem=recv, device_id=device, device_id_type=MESH
    )


class PlaneGather:
    def __init__(self, block, x_first, place, way, tp, sems, landed=None):
        self.block, self.x_first, self.way, self.tp = block, x_first, way, tp
        self.z, self.x = place
        self.s1, self.r1, self.s2, self.r2 = sems
        self.landed = landed
        self.waits = []

    def at(self, first_back, second_back):
        step = lambda value, back: lax.rem(value + 4 + 4 - back * self.way, 4)
        if self.x_first:
            return step(self.z, second_back) * N_X + step(self.x, first_back)
        return step(self.z, first_back) * N_X + step(self.x, second_back)

    def first(self, k):
        ref = self.block(self.at(k, 0))
        return remote(ref, ref, self.s1.at[k], self.r1.at[k], (self.at(-1, 0), self.tp))

    def second(self, k, b):
        ref = self.block(self.at(b, k))
        return remote(ref, ref, self.s2.at[4 * k + b], self.r2.at[4 * k + b], (self.at(0, -1), self.tp))

    def start(self):
        self.first(0).start()
        self.second(0, 0).start()
        if self.landed:
            self.landed(self.at(0, 0))

    def round(self, r):
        if r < 3:
            self.first(r).wait_recv()
            if r < 2:
                self.first(r + 1).start()
            self.second(0, r + 1).start()
            if self.landed:
                self.landed(self.at(r + 1, 0))
        for k in range(3):
            b = r - k
            if 0 <= b <= 3:
                self.second(k, b).wait_recv()
                if k < 2:
                    self.second(k + 1, b).start()
                if self.landed:
                    self.landed(self.at(b, k + 1))

    def drain(self):
        for k in range(3):
            self.first(k).wait_send()
            for b in range(4):
                self.second(k, b).wait_send()


def block_kernel(
    far_ref, cond_ref, cctx_ref, ws_ref, wc_ref, wg_ref, gain_ref, bias_ref, latent_ref, ctx_ref, wq_ref, wk_ref,
    wv_ref, wo_ref,
    out_ref,
    ada, part, total_x, total, got_x, got_z, mod, buf, w, wo, q, kv, lines, diag, table, stage, att,
    own_sem, sx, rx, sz, rz, sy, ry, s_ag, r_ag, s_sib, r_sib, s_halo, r_halo,
    c_s1, c_r1, c_s2, c_r2, a_s1, a_r1, a_s2, a_r2, b_s1, b_r1, b_s2, b_r2,
    s_wy, r_wy, s_wsa, r_wsa, s_wsb, r_wsb, s_wso, r_wso, s_at, r_at,
):
    sp, tp = lax.axis_index("sp"), lax.axis_index("tp")
    z, x = lax.div(sp, N_X), lax.rem(sp, N_X)
    y, c = lax.div(tp, 2), lax.rem(tp, 2)
    n_sp = N_X * N_Z
    way = 1 - 2 * c
    sib = 2 * y + 1 - c
    here = (sp, sib)
    cols = wq_ref.shape[1]
    width = buf.shape[2]
    tokens = buf.shape[1]
    y_at = lambda back: lax.rem(y + 8 - back * way, 4)
    y_next = (sp, 2 * y_at(-1) + c)

    own_lat = [pltpu.make_async_copy(latent_ref.at[s], buf.at[2 * tp + s], own_sem.at[s]) for s in range(2)]
    own_wo = pltpu.make_async_copy(wo_ref, wo.at[c, :, 0], own_sem.at[2])
    own_ctx = [pltpu.make_async_copy(ctx_ref.at[s], buf.at[16 + s], own_sem.at[3 + s]) for s in range(2)]
    own_w = [
        pltpu.make_async_copy(ref, w.at[:, pl.ds(cols * i, cols)], own_sem.at[5 + i])
        for i, ref in enumerate((wq_ref, wk_ref, wv_ref))
    ]
    for copy in own_lat + [own_wo] + own_ctx + own_w:
        copy.start()

    x_peers = [z * N_X + lax.rem(x + k, N_X) for k in range(1, N_X)]
    z_peers = [lax.rem(z + k, N_Z) * N_X + x for k in range(1, N_Z)]
    tp_peers = [lax.rem(tp + k, 8) for k in range(1, 8)]
    up, down = lax.rem(sp + 1, n_sp), lax.rem(sp + n_sp - 1, n_sp)
    barrier = pltpu.get_barrier_semaphore()
    peers = [(p, tp) for p in x_peers + z_peers + [up, down]] + [(sp, p) for p in tp_peers]
    for device in peers:
        pl.semaphore_signal(barrier, inc=1, device_id=device, device_id_type=MESH)

    ada[...] = jnp.zeros_like(ada)
    columns = pl.ds(pl.multiple_of(sp * 128, 128), 128)
    ada[0:2, :] = cond_ref[:, columns].astype(jnp.float32)
    ada[2:3, :] = cctx_ref[:, columns].astype(jnp.float32)
    value = ada[...]
    value = (value / (1.0 + jnp.exp(-value))).astype(jnp.bfloat16)
    part[...] = jnp.zeros_like(part)
    for i, ref in enumerate((ws_ref, wc_ref, wg_ref)):
        rows = jnp.dot(value, ref[...], preferred_element_type=jnp.float32)
        part[3 * i : 3 * i + 3, :] = rows[:3]
    pl.semaphore_wait(barrier, len(peers))

    sends_x = [remote(part, got_x.at[k], sx.at[k], rx.at[k], (p, tp)) for k, p in enumerate(x_peers)]
    for copy in sends_x:
        copy.start()

    def ag(k, s):
        ref = buf.at[2 * (2 * y_at(k) + c) + s]
        return remote(ref, ref, s_ag.at[2 * k + s], r_ag.at[2 * k + s], y_next)

    def to_sib(j, s):
        ref = buf.at[2 * (2 * y_at(j) + c) + s]
        return remote(ref, ref, s_sib.at[2 * j + s], r_sib.at[2 * j + s], here)

    def w_cross(d):
        return remote(
            wo.at[c, sp, 0], wo.at[c, sp, 4 - d], s_wy.at[d - 1], r_wy.at[d - 1], (sp, 2 * lax.rem(y + d, 4) + c)
        )

    def w_sib(at, rel, n, send, recv):
        ref = wo.at[c, at, pl.ds(rel, n)]
        return remote(ref, ref, send.at[at], recv.at[at], here)

    own_lat[0].wait()
    ag(0, 0).start()
    own_wo.wait()
    for d in range(1, 4):
        w_cross(d).start()
    own_lat[1].wait()
    ag(0, 1).start()
    for s in range(2):
        to_sib(0, s).start()
    w_own = remote(wo.at[c, :, 0], wo.at[c, :, 0], s_wso.at[0], r_wso.at[0], here)
    w_own.start()

    ctx_gather = PlaneGather(
        lambda at: kv.at[pl.ds(32 + 2 * at, 2)], True, (z, x), way, tp, (c_s1, c_r1, c_s2, c_r2)
    )
    wa_gather = PlaneGather(
        lambda at: wo.at[c, at, pl.ds(1, 2)], False, (z, x), way, tp, (a_s1, a_r1, a_s2, a_r2),
        lambda at: w_sib(at, 1, 2, s_wsa, r_wsa).start(),
    )
    wb_gather = PlaneGather(
        lambda at: wo.at[c, at, pl.ds(3, 1)], True, (z, x), way, tp, (b_s1, b_r1, b_s2, b_r2),
        lambda at: w_sib(at, 3, 1, s_wsb, r_wsb).start(),
    )

    heads = bias_ref.shape[0]
    lines[...] = jnp.zeros_like(lines)
    for h in range(heads):
        lines[16 * h : 16 * h + 15, 0:31] = bias_ref[h]
    lane = lax.broadcasted_iota(jnp.int32, (GRID_W, 128), 1)
    col = lax.broadcasted_iota(jnp.int32, (GRID_W, 128), 0)
    first_col = jnp.clip(col - WIN_COLS // 2, 0, GRID_W - WIN_COLS)
    key_col = lax.rem(lane, GRID_W)
    col_ok = (key_col >= first_col) & (key_col < first_col + WIN_COLS)

    def tile(i, carry):
        def rolled(at, shift):
            line = jnp.broadcast_to(lines[pl.ds(at, 1), :], (GRID_W, 128))
            return pltpu.roll(line, shift, 1, stride=1, stride_axis=0)

        before = 16 * lax.div(i, 16) + lax.rem(i + 15, 16)
        both = jnp.where(lane < GRID_W, rolled(before, 128 - WIN_COLS + 1), rolled(i, GRID_W - WIN_COLS + 1))
        diag[i] = jnp.where(col_ok, both * LOG2E, -jnp.inf)
        return carry

    value = part[...]
    for k, copy in enumerate(sends_x):
        copy.wait()
        value = value + got_x[k]
    total_x[...] = value
    sends_z = [remote(total_x, got_z.at[k], sz.at[k], rz.at[k], (p, tp)) for k, p in enumerate(z_peers)]
    for copy in sends_z:
        copy.start()

    lax.fori_loop(0, 16 * heads, tile, 0)

    value = total_x[...]
    for k, copy in enumerate(sends_z):
        copy.wait()
        value = value + got_z[k]
    total[...] = value
    mine = pl.ds(pl.multiple_of(tp * cols, cols), cols)
    sends_y = [remote(total, mod.at[:, mine], sy.at[k], ry.at[k], (sp, p)) for k, p in enumerate(tp_peers)]
    for copy in sends_y:
        copy.start()
    mod[:, mine] = value

    for s in range(2):
        ag(0, s).wait_recv()
        ag(1, s).start()
        to_sib(1, s).start()
    for d in range(1, 4):
        w_cross(d).wait_recv()
    wa_gather.start()
    wb_gather.start()
    for copy in sends_y:
        copy.wait()
    for copy in own_ctx + own_w:
        copy.wait()

    factor = HEAD_DIM ** (-0.5) * LOG2E

    def halo(slot, s):
        there = lax.rem(sp + n_sp + 2 * lax.div(slot, 4) - 1, n_sp)
        return remote(
            kv.at[16 * s + REACH + slot], kv.at[16 * s + lax.rem(slot + 12, 16)],
            s_halo.at[2 * slot + s], r_halo.at[2 * slot + s], (there, tp),
        )

    def step(i, carry):
        j = lax.div(lax.max(i - 1, 0), 2)
        s = lax.rem(lax.max(i - 1, 0), 2)
        slot_a = 2 * y_at(j) + c
        slot_b = 2 * y_at(-j) + 1 - c
        latents = i > 0

        @pl.when(i >= 5)
        def _():
            ag(j - 1, s).wait_recv()

        @pl.when((i >= 5) & (i < 7))
        def _():
            ag(j, s).start()

        @pl.when(i >= 5)
        def _():
            to_sib(j, s).start()

        for k, r in ((4, 0), (5, 1), (6, 2), (7, 3), (8, 4)):
            @pl.when(i == k)
            def _():
                ctx_gather.round(r)

        for k, r in ((3, 0), (5, 1), (7, 2)):
            @pl.when(i == k)
            def _():
                wa_gather.round(r)
                wb_gather.round(r)

        @pl.when(latents)
        def _():
            to_sib(j, s).wait_recv()

        zero = jnp.where(latents, 0, 1)
        at_a = zero * 16 + (1 - zero) * (2 * slot_a + s)
        at_b = zero * 17 + (1 - zero) * (2 * slot_b + s)
        which = zero * 2 + (1 - zero) * s
        lift = gain_ref[...] * (1.0 + mod[pl.ds(3 + which, 1), :])
        shift = mod[pl.ds(which, 1), :]
        hidden = []
        for at in (at_a, at_b):
            rows = buf[at].astype(jnp.float32)
            inverse = lax.rsqrt(jnp.mean(rows * rows, axis=-1, keepdims=True) + EPSILON)
            hidden.append((rows * inverse * lift + shift).astype(jnp.bfloat16))
        got = jnp.dot(jnp.concatenate(hidden, axis=0), w[...], preferred_element_type=jnp.float32)
        query = (got[:, :cols] * factor).astype(jnp.bfloat16)
        pair = got[:, cols:].astype(jnp.bfloat16)
        q_a = zero * 16 + (1 - zero) * (8 * s + slot_a)
        q_b = zero * 17 + (1 - zero) * (8 * s + slot_b)
        q[q_a] = query[:tokens]
        q[q_b] = query[tokens:]
        kv_a = zero * (32 + 2 * sp) + (1 - zero) * (16 * s + REACH + slot_a)
        kv_b = zero * (33 + 2 * sp) + (1 - zero) * (16 * s + REACH + slot_b)
        kv[kv_a] = pair[:tokens]
        kv[kv_b] = pair[tokens:]

        @pl.when(latents)
        def _():
            halo(slot_a, s).start()
            halo(slot_b, s).start()

        @pl.when(i == 0)
        def _():
            ctx_gather.start()

        return carry

    lax.fori_loop(0, 9, step, 0)

    def fill(i, carry):
        p, h = lax.div(i, heads), lax.rem(i, heads)
        g0 = 8 * sp + 2 * p
        start = jnp.clip(g0 - REACH, 0, 8 * n_sp - KEY_ROWS)
        for a in range(2):
            r0 = jnp.clip(g0 + a - REACH, 0, 8 * n_sp - WIN_ROWS)
            for v in range(0, KEY_ROWS, 2):
                e = jnp.clip(start - g0 - a + WIN_ROWS + v, 0, 15)
                row = start + v + lax.div(lane, GRID_W)
                ok = (row >= r0) & (row < r0 + WIN_ROWS)
                table[i, GRID_W * a : GRID_W * (a + 1), GRID_W * v : GRID_W * (v + 2)] = jnp.where(
                    ok, diag[16 * h + e], -jnp.inf
                )
        return carry

    lax.fori_loop(0, 4 * heads, fill, 0)

    def all_halos(i, carry):
        halo(lax.div(i, 2), lax.rem(i, 2)).wait_recv()
        return carry

    lax.fori_loop(0, 16, all_halos, 0)
    wa_gather.round(3)
    wb_gather.round(3)
    ctx_gather.round(5)

    contract = (((1,), (1,)), ((), ()))
    nq = 2 * GRID_W
    low = lax.broadcasted_iota(jnp.int32, (nq, 128), 1) < HEAD_DIM
    first_head = lax.broadcasted_iota(jnp.int32, (2 * nq, 1), 0) < nq

    def attended_to(idx, s, there):
        return remote(
            stage.at[idx, s, there], att.at[tp, s], s_at.at[4 * idx + 2 * s + there], r_at.at[2 * tp + s],
            (sp, 2 * lax.rem(y + 1 + idx, 4) + there),
        )

    def attend(t, carry):
        idx, s = lax.div(t, 2), lax.rem(t, 2)

        for k, r in ((1, 4), (4, 5)):
            @pl.when(t == k)
            def _():
                wa_gather.round(r)
                wb_gather.round(r)

        p = lax.rem(y + 1 + idx, 4)
        start = jnp.clip(8 * sp + 2 * p - REACH, 0, 8 * n_sp - KEY_ROWS) - (8 * sp - REACH)
        rows = pl.ds(16 * s + start, KEY_ROWS)
        outs = []
        for lp in range(2):
            lanes = slice(128 * lp, 128 * lp + 128)
            values = slice(cols + 128 * lp, cols + 128 * lp + 128)
            one = q[pl.ds(8 * s + 2 * p, 2), :, lanes].reshape(nq, 128)
            none = jnp.zeros_like(one)
            both = jnp.concatenate([jnp.where(low, one, none), jnp.where(low, none, one)], axis=0)
            key = kv[rows, :, lanes].reshape(-1, 128)
            val = kv[rows, :, values].reshape(-1, 128)
            near = lax.dot_general(both, key, contract, preferred_element_type=jnp.float32)
            bias = table[pl.ds(heads * p + 2 * lp, 2)].reshape(2 * nq, -1)
            near = near + bias
            far_rows = [kv.at[32 + 2 * u + s] for u in range(n_sp)]
            ckey = jnp.concatenate([ref[:, lanes] for ref in far_rows], axis=0)
            cval = jnp.concatenate([ref[:, values] for ref in far_rows], axis=0)
            far = lax.dot_general(both, ckey, contract, preferred_element_type=jnp.float32)
            lift = jnp.where(first_head, far_ref[2 * lp], far_ref[2 * lp + 1]) * LOG2E
            top = jnp.maximum(jnp.max(near, axis=-1, keepdims=True), jnp.max(far, axis=-1, keepdims=True) + lift)
            near = jnp.exp2(near - top).astype(jnp.bfloat16)
            far = jnp.exp2(far - (top - lift)).astype(jnp.bfloat16)
            got = jnp.dot(
                near, jnp.concatenate([val, jnp.ones_like(val)], axis=1), preferred_element_type=jnp.float32
            ) + jnp.dot(far, jnp.concatenate([cval, jnp.ones_like(cval)], axis=1), preferred_element_type=jnp.float32)
            got = got[:, :128] / got[:, 128:]
            outs.append(jnp.where(low, got[:nq], got[nq:]).astype(jnp.bfloat16))
        done = jnp.concatenate(outs, axis=1)
        stage[idx, s, 0] = done[:GRID_W]
        stage[idx, s, 1] = done[GRID_W:]

        @pl.when(idx < 3)
        def _():
            attended_to(idx, s, 0).start()
            attended_to(idx, s, 1).start()

        @pl.when(idx == 3)
        def _():
            attended_to(idx, s, 1 - c).start()
            att[tp, s] = stage[idx, s, c]

        return carry

    lax.fori_loop(0, 8, attend, 0)

    def from_sib(i, carry):
        ref = wo.at[c, i, pl.ds(1, 2)]
        remote(ref, ref, s_wsa.at[i], r_wsa.at[i], here).wait_recv()
        ref = wo.at[c, i, pl.ds(3, 1)]
        remote(ref, ref, s_wsb.at[i], r_wsb.at[i], here).wait_recv()
        return carry

    lax.fori_loop(0, 16, from_sib, 0)
    w_own.wait_recv()

    def from_peer(k, carry):
        src = lax.rem(tp + k, 8)
        for s in range(2):
            remote(stage.at[0, s, 0], att.at[src, s], s_at.at[0], r_at.at[2 * src + s], here).wait_recv()
        return carry

    lax.fori_loop(1, 8, from_peer, 0)

    def project(n, carry):
        at = pl.ds(pl.multiple_of(512 * n, 512), 512)
        acc = jnp.zeros((2 * tokens, 512), jnp.float32)
        for core in range(2):
            for rel in range(4):
                rows = att[2 * lax.rem(y + rel, 4) + core].reshape(2 * tokens, cols)
                weight = wo[core, :, rel, :, at].reshape(cols, 512)
                acc = acc + jnp.dot(rows, weight, preferred_element_type=jnp.float32)
        for s in range(2):
            mixed = buf[2 * tp + s, :, at].astype(jnp.float32) + mod[6 + s : 7 + s, at] * acc[s * tokens : (s + 1) * tokens]
            out_ref[s, :, at] = mixed.astype(jnp.bfloat16)
        return carry

    lax.fori_loop(0, width // 512, project, 0)

    for k in range(3):
        for s in range(2):
            ag(k, s).wait_send()
    for j in range(4):
        for s in range(2):
            to_sib(j, s).wait_send()
    for d in range(1, 4):
        w_cross(d).wait_send()
    w_own.wait_send()
    for gather in (ctx_gather, wa_gather, wb_gather):
        gather.drain()

    def drain(i, carry):
        halo(lax.div(i, 2), lax.rem(i, 2)).wait_send()
        w_sib(i, 1, 2, s_wsa, r_wsa).wait_send()
        w_sib(i, 3, 1, s_wsb, r_wsb).wait_send()
        return carry

    lax.fori_loop(0, 16, drain, 0)
    for idx in range(3):
        for s in range(2):
            for there in range(2):
                attended_to(idx, s, there).wait_send()
    for s in range(2):
        attended_to(3, s, 1 - c).wait_send()


def on_device(
    latent, context, cond, ctx_cond, w_shift, w_scale, w_gate, norm_gain,
    w_query, w_key, w_value, w_out, rel_bias, ctx_bias,
):
    samples, tokens, width = latent.shape
    cols = w_query.shape[1]
    heads = cols // HEAD_DIM
    n_sp = N_X * N_Z
    vmem, anywhere = pl.BlockSpec(memory_space=pltpu.VMEM), pl.BlockSpec(memory_space=pl.ANY)
    f32, bf16 = jnp.float32, jnp.bfloat16
    dma = lambda n: pltpu.SemaphoreType.DMA((n,))
    sems = [8, 3, 3, 3, 3, 7, 7, 6, 6, 8, 8, 16, 16]
    sems += [3, 3, 12, 12] * 3
    sems += [3, 3, 16, 16, 16, 16, 1, 1, 16, 16]
    return pl.pallas_call(
        block_kernel,
        out_shape=jax.ShapeDtypeStruct(latent.shape, bf16),
        in_specs=[pl.BlockSpec(memory_space=pltpu.SMEM)] + [vmem] * 7 + [anywhere] * 6,
        out_specs=vmem,
        scratch_shapes=[
            pltpu.VMEM((8, 128), f32),
            pltpu.VMEM((16, cols), f32),
            pltpu.VMEM((16, cols), f32),
            pltpu.VMEM((16, cols), f32),
            pltpu.VMEM((3, 16, cols), f32),
            pltpu.VMEM((3, 16, cols), f32),
            pltpu.VMEM((16, width), f32),
            pltpu.VMEM((18, tokens, width), bf16),
            pltpu.VMEM((width, 3 * cols), bf16),
            pltpu.VMEM((2, n_sp, N_Y, 16, width), bf16),
            pltpu.VMEM((18, tokens, cols), bf16),
            pltpu.VMEM((32 + 2 * n_sp, tokens, 2 * cols), bf16),
            pltpu.VMEM((16 * heads, 128), f32),
            pltpu.VMEM((16 * heads, GRID_W, 128), f32),
            pltpu.VMEM((4 * heads, 2 * GRID_W, KEY_ROWS * GRID_W), f32),
            pltpu.VMEM((4, samples, 2, tokens, cols), bf16),
            pltpu.VMEM((8, samples, tokens, cols), bf16),
        ]
        + [dma(n) for n in sems],
        compiler_params=pltpu.CompilerParams(
            collective_id=1, has_side_effects=True, vmem_limit_bytes=60 * 2**20
        ),
    )(
        ctx_bias, cond, ctx_cond[None, :], w_shift, w_scale, w_gate, norm_gain[None, :], rel_bias,
        latent, context, w_query, w_key, w_value, w_out.reshape(n_sp, 16, width),
    )


def solution(mesh):
    return jax.shard_map(
        on_device,
        mesh=mesh,
        in_specs=(
            P(None, ("sp", "tp"), None),
            P(None, "sp", None),
            P(),
            P(),
            P("sp", "tp"),
            P("sp", "tp"),
            P("sp", "tp"),
            P(),
            P(None, "tp"),
            P(None, "tp"),
            P(None, "tp"),
            P("tp", None),
            P("tp", None, None),
            P("tp"),
        ),
        out_specs=P(None, ("sp", "tp"), None),
        check_vma=False,
    )
```

time: 247 us -> 95.2 us (0.39); the launches traced: 244 us -> 94.9 us
  waiting for transfers between devices: 92 us -> 0 us
  blocking collectives: 90.2 us -> 0 us
  Pallas kernels: 12.2 us -> 90.4 us
  matrix products: 15.8 us -> 0 us
  between operations: 13.2 us -> 0.01 us
  other arithmetic: 10.1 us -> 0 us
  starting transfers between devices: 5.3 us -> 0 us
    pallas_call x1, Pallas kernels: 12.2 us -> 90.4 us  [on_device(): pl.pallas_call(block_kernel, out_shape=jax.ShapeDtypeStruct(latent.shape,...]
    psum x1 -> x0, blocking collectives: 62.2 us -> none  [on_device(): summed = lax.psum(partial_value, 'sp')]
    all_gather x2 -> x0, waiting for transfers between devices: 43.5 us -> none  [the longest x1 24 us: on_device(): lax.all_gather(hidden, 'tp', axis=1, tiled=True)]
    reduce_scatter x1 -> x0, waiting for transfers between devices: 36 us -> none  [on_device(): lax.psum_scatter(jnp.einsum('tsc,cd->tsd', attended, w_out, preferred_ele...]
    all_gather x1 -> x0, blocking collectives: 28 us -> none  [on_device(): modulation = lax.all_gather(summed, 'tp', axis=2, tiled=True)]
    dot_general x6 -> x0, matrix products: 15.8 us -> none  [the longest x1 6.2 us: on_device(): jnp.dot(lax.all_gather(hidden, 'tp', axis=1, tiled=True), w_triple, prefe...]
    ppermute x2 -> x0, waiting for transfers between devices: 12.4 us -> none  [the longest x1 8.41 us: extended(): before = lax.ppermute(last, axis, up)]
    ppermute x2 -> x0, starting transfers between devices: 5.18 us -> none  [the longest x1 3.9 us: extended(): before = lax.ppermute(last, axis, up)]
  transfers between devices with their start and end apart: 5 -> 0, of which waited for: 5 -> 0; matrix products, arithmetic and copies ran while one was open for 6% -> 0% of each run, Pallas kernels for 0% -> 0%
where the time goes in v1:
time: 95.2 us; the launch traced here: 94.9 us
  Pallas kernels  90.4 us (95%)
  local copies, waits for them, and re-layouts  4.54 us (5%)
    pallas_call x1, Pallas kernels, on_device(): pl.pallas_call(block_kernel, out_shape=jax.ShapeDtypeStruct(latent.shape,...  90.4 us
    unnamed x2, local copies, waits for them, and re-layouts  3.25 us

profile of v1, /device:TPU:1, one launch (start us, length us, event | category | flops | bytes accessed | tf_op | source)
XLA Modules:
  0.0 94.9 jit_solution(18359035992717021733)
XLA Ops:
  0.0 1.3 %broadcast_in_dim.6.cctx_ref = bf16[1,2048]{1,0:T(2,128)(2,1)} reshape(bf16[2048]{0:T(1024)(128)(2,1)} %param.17) | data formatting | bytes 8192 | tf_op jit(solution)/shard_map/broadcast_in_dim | solution.py:509
  1.3 1.4 %copy.15.bias_ref = f32[4,15,31]{2,1,0:T(8,128)} copy(f32[4,15,31]{2,0,1:T(4,128)} %param.26) | data formatting | bytes 14880 | tf_op args[12]
  2.7 90.4 %shard_map.136 = bf16[2,64,2048]{2,1,0:T(8,128)(2,1)} custom-call(f32[4]{0:T(128)} %far_ref.1, bf16[2,2048]{1,0:T(2,128)(2,1)} %cond_ref.1, bf16[1,2048]{1,0:T(2,128)(2,1)} %broadcast_in_dim.6.cctx_ref, bf16[128,256]{1,0:T(8,128)(2,1)} %ws_ref.1, bf16[128,256]{1,0:T(8,128)(2,1)} %wc_ref.1, bf16[128,256]{1,0:T(8,128)(2,1)} %wg_ref.1, f32[1,2048]{1,0:T(1,128)} %bitcast.3, ...), custom_call_target="tpu_custom_call" | custom-call | tf_op jit(solution)/shard_map/pallas_call | solution.py:480
  93.0 1.9 %copy.17 = bf16[2,64,2048]{2,1,0:T(8,128)(2,1)} copy(bf16[2,64,2048]{2,1,0:T(8,128)(2,1)} %shard_map.136) | data formatting | bytes 1048576

commit v2 on v1

v2 whole, which is shorter than its diff:
```python
import functools

import jax
import jax.numpy as jnp
from jax import lax
from jax.experimental import pallas as pl
from jax.experimental.pallas import tpu as pltpu
from jax.sharding import PartitionSpec as P

HEAD_DIM = 64
GRID_W = 64
WIN_ROWS = 8
WIN_COLS = 16
EPSILON = 1e-06
LOG2E = 1.4426950408889634
MESH = pl.DeviceIdType.MESH

N_X, N_Z, N_Y = 4, 4, 4
PAD_ROWS = 16
KEY_ROWS = 10
REACH = WIN_ROWS // 2


def remote(src, dst, send, recv, device):
    return pltpu.make_async_remote_copy(
        src_ref=src, dst_ref=dst, send_sem=send, recv_sem=recv, device_id=device, device_id_type=MESH
    )


class PlaneGather:
    HOPS = (0, 1, 1, 2)
    BACK = (0, 1, -1, 2)
    COUNTS = (4, 6, 4, 1)

    def __init__(self, block, x_first, place, way, tp, send, recv, landed=None):
        self.block, self.x_first, self.way, self.tp = block, x_first, way, tp
        self.z, self.x = place
        self.send, self.recv = send, recv
        self.landed = landed

    def at(self, first_back, second_back):
        step = lambda value, back: lax.rem(value + 8 - back * self.way, 4)
        if self.x_first:
            return step(self.z, second_back) * N_X + step(self.x, first_back)
        return step(self.z, first_back) * N_X + step(self.x, second_back)

    def pass_on(self, b, k, hops, first=0, second=0):
        ref = self.block(self.at(self.BACK[b], self.BACK[k]))
        remote(ref, ref, self.send, self.recv.at[hops - 1], (self.at(-first, -second), self.tp)).start()

    def have(self, b, k):
        hops = self.HOPS[b] + self.HOPS[k]
        if k == 0:
            if b == 0:
                self.pass_on(b, k, 1, first=1)
                self.pass_on(b, k, 1, first=-1)
            if b == 1:
                self.pass_on(b, k, 2, first=1)
            self.pass_on(b, k, hops + 1, second=1)
            self.pass_on(b, k, hops + 1, second=-1)
        if k == 1:
            self.pass_on(b, k, hops + 1, second=1)
        if self.landed:
            self.landed(self.at(self.BACK[b], self.BACK[k]))

    def start(self):
        self.have(0, 0)

    def round(self, r):
        for b, k in ((1, 0), (0, 1), (1, 1), (2, 0), (3, 0), (2, 1), (0, 2), (0, 3), (1, 2), (2, 2), (1, 3), (2, 3), (3, 1), (3, 2), (3, 3)):
            if self.HOPS[b] + self.HOPS[k] == r + 1:
                self.have(b, k)


def took(ref, sem):
    pltpu.make_async_copy(ref, ref, sem).wait()


def block_kernel(
    far_ref, cond_hbm, cctx_hbm, ws_ref, wc_ref, wg_ref, gain_hbm, bias_hbm, latent_ref, ctx_ref, wq_ref, wk_ref,
    wv_ref, wo_ref,
    out_ref,
    cond_ref, cctx_ref, w_mod, gain_ref, bias_ref,
    ada, part, total_x, total, got_x, got_z, mod, buf, w, wo, q, kv, lines, diag, table, stage, att, out_buf,
    own_sem, sx, rx, sz, rz, sy, ry, s_ag, r_ag, s_sib, r_sib, s_halo, r_halo, s_ctx, r_ctx, s_w, r_w,
    s_wy, r_wy, s_ws, r_ws, s_yr, r_yr, s_ys, r_ys, s_at, r_at, out_sem,
):
    sp, tp = lax.axis_index("sp"), lax.axis_index("tp")
    z, x = lax.div(sp, N_X), lax.rem(sp, N_X)
    y, c = lax.div(tp, 2), lax.rem(tp, 2)
    n_sp = N_X * N_Z
    way = 1 - 2 * c
    sib = 2 * y + 1 - c
    here = (sp, sib)
    cols = wq_ref.shape[1]
    share = 512
    width = buf.shape[2]
    tokens = buf.shape[1]
    y_at = lambda back: lax.rem(y + 8 - back * way, 4)
    y_next = (sp, 2 * y_at(-1) + c)

    x_peers = [z * N_X + lax.rem(x + k, N_X) for k in range(1, N_X)]
    z_peers = [lax.rem(z + k, N_Z) * N_X + x for k in range(1, N_Z)]
    tp_peers = [lax.rem(tp + k, 8) for k in range(1, 8)]
    up, down = lax.rem(sp + 1, n_sp), lax.rem(sp + n_sp - 1, n_sp)
    barrier = pltpu.get_barrier_semaphore()
    peers = [(p, tp) for p in x_peers + z_peers + [up, down]] + [(sp, p) for p in tp_peers]
    for device in peers:
        pl.semaphore_signal(barrier, inc=1, device_id=device, device_id_type=MESH)

    small = [
        pltpu.make_async_copy(src, dst, own_sem.at[8 + i])
        for i, (src, dst) in enumerate(
            ((cond_hbm, cond_ref), (cctx_hbm, cctx_ref), (ws_ref, w_mod.at[0]), (wc_ref, w_mod.at[1]), (wg_ref, w_mod.at[2]))
        )
    ]
    later = [pltpu.make_async_copy(gain_hbm, gain_ref, own_sem.at[13]), pltpu.make_async_copy(bias_hbm, bias_ref, own_sem.at[14])]
    own_lat = [pltpu.make_async_copy(latent_ref.at[s], buf.at[2 * tp + s], own_sem.at[s]) for s in range(2)]
    own_wo = pltpu.make_async_copy(wo_ref, wo.at[c, :, 0], own_sem.at[2])
    own_ctx = [pltpu.make_async_copy(ctx_ref.at[s], buf.at[16 + s], own_sem.at[3 + s]) for s in range(2)]
    own_w = [
        pltpu.make_async_copy(ref, w.at[:, pl.ds(cols * i, cols)], own_sem.at[5 + i])
        for i, ref in enumerate((wq_ref, wk_ref, wv_ref))
    ]
    for copy in small + own_lat + later + [own_wo] + own_ctx + own_w:
        copy.start()

    ada[...] = jnp.zeros_like(ada)
    part[...] = jnp.zeros_like(part)
    for s in range(2):
        kv[16 * s + 15] = jnp.zeros(kv.shape[1:], kv.dtype)
    columns = pl.ds(pl.multiple_of(sp * 128, 128), 128)
    for copy in small:
        copy.wait()
    ada[0:2, :] = cond_ref[:, columns].astype(jnp.float32)
    both = cctx_ref[pl.ds(pl.multiple_of(lax.div(sp, 2) * 256, 256), 256)].astype(jnp.float32).reshape(1, 256)
    ada[2:3, :] = jnp.where(lax.rem(sp, 2) == 0, both[:, :128], both[:, 128:])
    value = ada[...]
    value = (value / (1.0 + jnp.exp(-value))).astype(jnp.bfloat16)
    for i in range(3):
        rows = jnp.dot(value, w_mod[i], preferred_element_type=jnp.float32)
        part[3 * i : 3 * i + 3, :] = rows[:3]
    pl.semaphore_wait(barrier, len(peers))

    for k, p in enumerate(x_peers):
        remote(part, got_x.at[k], sx.at[0], rx.at[0], (p, tp)).start()

    def ag(k, s):
        ref = buf.at[2 * (2 * y_at(k) + c) + s]
        return remote(ref, ref, s_ag.at[0], r_ag.at[2 * k + s], y_next)

    def to_sib(j, s):
        ref = buf.at[2 * (2 * y_at(j) + c) + s]
        return remote(ref, ref, s_sib.at[0], r_sib.at[2 * j + s], here)

    def relay(k, s):
        ag(k, s).wait_recv()
        if k < 2:
            ag(k + 1, s).start()
        to_sib(k + 1, s).start()

    front, back = pl.ds(0, share), pl.ds(share, width - share)

    def w_cross(d):
        return remote(
            wo.at[c, sp, 0, :, front], wo.at[c, sp, 4 - d, :, front], s_wy.at[0], r_wy.at[0],
            (sp, 2 * lax.rem(y + d, 4) + c),
        )

    def w_ring(k, h):
        ref = lambda at: wo.at[c, pl.ds(4 * h, 4), lax.rem(8 - at * way, 4), :, back]
        return remote(ref(k), ref(k + 1), s_yr.at[0], r_yr.at[4 * k + h], y_next)

    def w_ring_sib(k, h):
        ref = wo.at[c, pl.ds(4 * h, 4), lax.rem(8 - k * way, 4), :, back]
        return remote(ref, ref, s_ys.at[0], r_ys.at[0], here)

    def w_ring_round(k, h):
        w_ring(k, h).wait_recv()
        if k < 2:
            w_ring(k + 1, h).start()
        w_ring_sib(k + 1, h).start()

    def w_sib(rel, n):
        def landed(at):
            ref = wo.at[c, at, pl.ds(rel, n), :, front]
            remote(ref, ref, s_ws.at[0], r_ws.at[0], here).start()

        return landed

    for s in range(2):
        own_lat[s].wait()
        ag(0, s).start()
    own_wo.wait()
    for s in range(2):
        to_sib(0, s).start()
    w_own = remote(wo.at[c, :, 0], wo.at[c, :, 0], s_ws.at[1], r_ws.at[1], here)
    w_own.start()

    ctx_gathers = [
        PlaneGather(lambda at: kv.at[32 + 2 * at], True, (z, x), way, tp, s_ctx.at[0], r_ctx),
        PlaneGather(lambda at: kv.at[33 + 2 * at], False, (z, x), way, tp, s_ctx.at[0], r_ctx),
    ]
    w_gathers = [
        PlaneGather(
            lambda at: wo.at[c, at, pl.ds(1, 2), :, front], False, (z, x), way, tp, s_w.at[0], r_w, w_sib(1, 2)
        ),
        PlaneGather(
            lambda at: wo.at[c, at, pl.ds(3, 1), :, front], True, (z, x), way, tp, s_w.at[0], r_w, w_sib(3, 1)
        ),
    ]

    def ctx_round(r):
        took(kv.at[pl.ds(0, 2 * PlaneGather.COUNTS[r])], r_ctx.at[r])
        for gather in ctx_gathers:
            gather.round(r)

    def w_round(r):
        took(wo.at[c, pl.ds(0, PlaneGather.COUNTS[r]), pl.ds(1, 3), :, front], r_w.at[r])
        for gather in w_gathers:
            gather.round(r)

    heads = bias_ref.shape[1]
    lines[...] = jnp.zeros_like(lines)
    for copy in later:
        copy.wait()
    for h in range(heads):
        lines[16 * h : 16 * h + 15, 0:31] = bias_ref[:, h, :]
    lines[...] = pltpu.roll(lines[...], 1, 0) + pltpu.roll(lines[...], GRID_W, 1)
    lane = lax.broadcasted_iota(jnp.int32, (GRID_W, 128), 1)
    col = lax.broadcasted_iota(jnp.int32, (GRID_W, 128), 0)
    first_col = jnp.clip(col - WIN_COLS // 2, 0, GRID_W - WIN_COLS)
    key_col = lax.rem(lane, GRID_W)
    col_ok = (key_col >= first_col) & (key_col < first_col + WIN_COLS)

    def tile(i, carry):
        line = jnp.broadcast_to(lines[pl.ds(i, 1), :], (GRID_W, 128))
        both = pltpu.roll(line, 128 - WIN_COLS + 1, 1, stride=1, stride_axis=0)
        diag[i] = jnp.where(col_ok, both * LOG2E, -jnp.inf)
        return carry

    took(got_x, sx.at[0])
    took(got_x, rx.at[0])
    total_x[...] = part[...] + got_x[0] + got_x[1] + got_x[2]
    for k, p in enumerate(z_peers):
        remote(total_x, got_z.at[k], sz.at[0], rz.at[0], (p, tp)).start()
    lax.fori_loop(0, 8 * heads, tile, 0, unroll=4)
    took(got_z, sz.at[0])
    took(got_z, rz.at[0])
    value = total_x[...] + got_z[0] + got_z[1] + got_z[2]
    total[...] = value
    mine = pl.ds(pl.multiple_of(tp * cols, cols), cols)
    for k, p in enumerate(tp_peers):
        remote(total, mod.at[:, mine], sy.at[0], ry.at[0], (sp, p)).start()
    mod[:, mine] = value
    relay(0, 0)
    lax.fori_loop(8 * heads, 16 * heads, tile, 0, unroll=4)
    relay(0, 1)
    for d in range(1, 4):
        w_cross(d).start()
    for copy in own_ctx + own_w:
        copy.wait()
    took(mod.at[:, pl.ds(0, 7 * cols)], sy.at[0])
    took(mod.at[:, pl.ds(0, 7 * cols)], ry.at[0])

    factor = HEAD_DIM ** (-0.5) * LOG2E

    def halo(slot, s):
        there = lax.rem(sp + n_sp + 2 * lax.div(slot, 4) - 1, n_sp)
        return remote(
            kv.at[16 * s + REACH + slot], kv.at[16 * s + lax.rem(slot + 12, 16)],
            s_halo.at[0], r_halo.at[0], (there, tp),
        )

    def halos(j):
        for slot in (2 * y_at(j) + c, 2 * y_at(-j) + 1 - c):
            @pl.when(slot != 3)
            def _():
                for s in range(2):
                    halo(slot, s).start()

    def step(i, carry):
        j = lax.div(lax.max(i - 1, 0), 2)
        s = lax.rem(lax.max(i - 1, 0), 2)
        slot_a = 2 * y_at(j) + c
        slot_b = 2 * y_at(-j) + 1 - c
        latents = i > 0

        for at, k, half in ((1, 1, 0), (3, 1, 1), (7, 2, 0), (8, 2, 1)):
            @pl.when(i == at)
            def _():
                relay(k, half)

        @pl.when(latents)
        def _():
            to_sib(j, s).wait_recv()

        zero = jnp.where(latents, 0, 1)
        at_a = zero * 16 + (1 - zero) * (2 * slot_a + s)
        at_b = zero * 17 + (1 - zero) * (2 * slot_b + s)
        which = zero * 2 + (1 - zero) * s
        lift = gain_ref[...] * (1.0 + mod[pl.ds(3 + which, 1), :])
        shift = mod[pl.ds(which, 1), :]
        hidden = []
        for at in (at_a, at_b):
            rows = buf[at].astype(jnp.float32)
            inverse = lax.rsqrt(jnp.mean(rows * rows, axis=-1, keepdims=True) + EPSILON)
            hidden.append((rows * inverse * lift + shift).astype(jnp.bfloat16))
        got = jnp.dot(jnp.concatenate(hidden, axis=0), w[...], preferred_element_type=jnp.float32)
        query = (got[:, :cols] * factor).astype(jnp.bfloat16)
        pair = got[:, cols:].astype(jnp.bfloat16)
        q_a = zero * 16 + (1 - zero) * (8 * s + slot_a)
        q_b = zero * 17 + (1 - zero) * (8 * s + slot_b)
        q[q_a] = query[:tokens]
        q[q_b] = query[tokens:]
        kv_a = zero * (32 + 2 * sp) + (1 - zero) * (16 * s + REACH + slot_a)
        kv_b = zero * (33 + 2 * sp) + (1 - zero) * (16 * s + REACH + slot_b)
        kv[kv_a] = pair[:tokens]
        kv[kv_b] = pair[tokens:]

        @pl.when(i == 0)
        def _():
            for gather in ctx_gathers:
                gather.start()

        @pl.when(i == 4)
        def _():
            for h in range(4):
                w_ring(0, h).start()
            ctx_round(0)
            halos(0)

        @pl.when(i == 6)
        def _():
            halos(1)

        @pl.when(i == 8)
        def _():
            ctx_round(1)
            halos(2)
            halos(3)

        return carry

    lax.fori_loop(0, 9, step, 0)

    def fill(i, carry):
        p, h = lax.div(i, heads), lax.rem(i, heads)
        g0 = 8 * sp + 2 * p
        start = jnp.clip(g0 - REACH, 0, 8 * n_sp - KEY_ROWS)
        for a in range(2):
            r0 = jnp.clip(g0 + a - REACH, 0, 8 * n_sp - WIN_ROWS)
            for v in range(0, KEY_ROWS, 2):
                e = jnp.clip(start - g0 - a + WIN_ROWS + v, 0, 15)
                row = start + v + lax.div(lane, GRID_W)
                ok = (row >= r0) & (row < r0 + WIN_ROWS)
                table[i, GRID_W * a : GRID_W * (a + 1), GRID_W * v : GRID_W * (v + 2)] = jnp.where(
                    ok, diag[16 * h + e], -jnp.inf
                )
        return carry

    lax.fori_loop(0, 4 * heads, fill, 0)
    took(wo.at[c, 0, pl.ds(1, 3), :, front], r_wy.at[0])
    w_ring_round(0, 0)
    w_ring_round(0, 1)
    ctx_round(2)
    for gather in w_gathers:
        gather.start()
    w_ring_round(0, 2)
    w_ring_round(0, 3)
    ctx_round(3)
    took(kv.at[pl.ds(0, 14)], r_halo.at[0])

    contract = (((1,), (1,)), ((), ()))
    nq = 2 * GRID_W
    low = lax.broadcasted_iota(jnp.int32, (nq, 128), 1) < HEAD_DIM
    first_head = lax.broadcasted_iota(jnp.int32, (2 * nq, 1), 0) < nq

    def attended_to(idx, s, there):
        return remote(
            stage.at[idx, s, there], att.at[tp, s], s_at.at[0], r_at.at[0],
            (sp, 2 * lax.rem(y + 1 + idx, 4) + there),
        )

    def attend(t, carry):
        idx, s = lax.div(t, 2), lax.rem(t, 2)

        p = lax.rem(y + 1 + idx, 4)
        start = jnp.clip(8 * sp + 2 * p - REACH, 0, 8 * n_sp - KEY_ROWS) - (8 * sp - REACH)
        rows = pl.ds(16 * s + start, KEY_ROWS)
        outs = []
        for lp in range(2):
            lanes = slice(128 * lp, 128 * lp + 128)
            values = slice(cols + 128 * lp, cols + 128 * lp + 128)
            one = q[pl.ds(8 * s + 2 * p, 2), :, lanes].reshape(nq, 128)
            none = jnp.zeros_like(one)
            both = jnp.concatenate([jnp.where(low, one, none), jnp.where(low, none, one)], axis=0)
            key = kv[rows, :, lanes].reshape(-1, 128)
            val = kv[rows, :, values].reshape(-1, 128)
            near = lax.dot_general(both, key, contract, preferred_element_type=jnp.float32)
            bias = table[pl.ds(heads * p + 2 * lp, 2)].reshape(2 * nq, -1)
            near = near + bias
            far_rows = [kv.at[32 + 2 * u + s] for u in range(n_sp)]
            ckey = jnp.concatenate([ref[:, lanes] for ref in far_rows], axis=0)
            cval = jnp.concatenate([ref[:, values] for ref in far_rows], axis=0)
            far = lax.dot_general(both, ckey, contract, preferred_element_type=jnp.float32)
            lift = jnp.where(first_head, far_ref[2 * lp], far_ref[2 * lp + 1]) * LOG2E
            top = jnp.maximum(jnp.max(near, axis=-1, keepdims=True), jnp.max(far, axis=-1, keepdims=True) + lift)
            near = jnp.exp2(near - top).astype(jnp.bfloat16)
            far = jnp.exp2(far - (top - lift)).astype(jnp.bfloat16)
            got = jnp.dot(
                near, jnp.concatenate([val, jnp.ones_like(val)], axis=1), preferred_element_type=jnp.float32
            ) + jnp.dot(far, jnp.concatenate([cval, jnp.ones_like(cval)], axis=1), preferred_element_type=jnp.float32)
            got = got[:, :128] / got[:, 128:]
            outs.append(jnp.where(low, got[:nq], got[nq:]).astype(jnp.bfloat16))
        done = jnp.concatenate(outs, axis=1)
        stage[idx, s, 0] = done[:GRID_W]
        stage[idx, s, 1] = done[GRID_W:]

        @pl.when(idx < 3)
        def _():
            attended_to(idx, s, 0).start()
            attended_to(idx, s, 1).start()

        @pl.when(idx == 3)
        def _():
            attended_to(idx, s, 1 - c).start()
            att[tp, s] = stage[idx, s, c]

        for at, k, h in ((0, 1, 0), (1, 1, 1), (2, 1, 2), (3, 1, 3), (4, 2, 0), (5, 2, 1), (6, 2, 2), (7, 2, 3)):
            @pl.when(t == at)
            def _():
                w_ring_round(k, h)

        for at, r in ((1, 0), (3, 1), (5, 2), (7, 3)):
            @pl.when(t == at)
            def _():
                w_round(r)

        return carry

    lax.fori_loop(0, 8, attend, 0)

    took(wo.at[1 - c, :, pl.ds(1, 3), :, front], r_ws.at[0])
    took(wo.at[1 - c, :, 0], r_ws.at[1])
    took(wo.at[1 - c, :, pl.ds(1, 3), :, back], r_ys.at[0])
    took(att.at[pl.ds(0, 7)], r_at.at[0])

    def project(n, carry):
        at = pl.ds(pl.multiple_of(512 * n, 512), 512)
        acc = jnp.zeros((2 * tokens, 512), jnp.float32)
        for core in range(2):
            for rel in range(4):
                rows = att[2 * lax.rem(y + rel, 4) + core].reshape(2 * tokens, cols)
                weight = wo[core, :, rel, :, at].reshape(cols, 512)
                acc = acc + jnp.dot(rows, weight, preferred_element_type=jnp.float32)
        for s in range(2):
            mixed = buf[2 * tp + s, :, at].astype(jnp.float32) + mod[6 + s : 7 + s, at] * acc[s * tokens : (s + 1) * tokens]
            out_buf[s, :, at] = mixed.astype(jnp.bfloat16)
        pltpu.make_async_copy(out_buf.at[:, :, at], out_ref.at[:, :, at], out_sem.at[n]).start()
        return carry

    lax.fori_loop(0, width // 512, project, 0)

    took(buf.at[pl.ds(0, 6)], s_ag.at[0])
    took(buf.at[pl.ds(0, 8)], s_sib.at[0])
    took(kv.at[pl.ds(0, 14)], s_halo.at[0])
    took(kv.at[pl.ds(0, 30)], s_ctx.at[0])
    took(wo.at[c, pl.ds(0, 15), pl.ds(1, 3), :, front], s_w.at[0])
    took(wo.at[c, 0, pl.ds(1, 3), :, front], s_wy.at[0])
    took(wo.at[c, :, pl.ds(1, 3), :, front], s_ws.at[0])
    took(wo.at[c, :, 0], s_ws.at[1])
    took(wo.at[c, :, pl.ds(1, 3), :, back], s_yr.at[0])
    took(wo.at[c, :, pl.ds(1, 3), :, back], s_ys.at[0])
    took(att.at[pl.ds(0, 7)], s_at.at[0])
    for n in range(width // 512):
        at = pl.ds(512 * n, 512)
        pltpu.make_async_copy(out_buf.at[:, :, at], out_ref.at[:, :, at], out_sem.at[n]).wait()


def on_device(
    latent, context, cond, ctx_cond, w_shift, w_scale, w_gate, norm_gain,
    w_query, w_key, w_value, w_out, rel_bias, ctx_bias,
):
    samples, tokens, width = latent.shape
    cols = w_query.shape[1]
    heads = cols // HEAD_DIM
    n_sp = N_X * N_Z
    anywhere = pl.BlockSpec(memory_space=pl.ANY)
    f32, bf16 = jnp.float32, jnp.bfloat16
    dma = lambda n: pltpu.SemaphoreType.DMA((n,))
    sems = [15, 1, 1, 1, 1, 1, 1, 1, 6, 1, 8, 1, 1, 1, 4, 1, 4]
    sems += [1, 1, 2, 2, 1, 12, 1, 1, 1, 1, 4]
    return pl.pallas_call(
        block_kernel,
        out_shape=jax.ShapeDtypeStruct(latent.shape, bf16),
        in_specs=[pl.BlockSpec(memory_space=pltpu.SMEM)] + [anywhere] * 13,
        out_specs=anywhere,
        scratch_shapes=[
            pltpu.VMEM(cond.shape, bf16),
            pltpu.VMEM(ctx_cond.shape, bf16),
            pltpu.VMEM((3,) + w_shift.shape, bf16),
            pltpu.VMEM((1, width), f32),
            pltpu.VMEM((15, heads, 31), f32),
            pltpu.VMEM((8, 128), f32),
            pltpu.VMEM((16, cols), f32),
            pltpu.VMEM((16, cols), f32),
            pltpu.VMEM((16, cols), f32),
            pltpu.VMEM((3, 16, cols), f32),
            pltpu.VMEM((3, 16, cols), f32),
            pltpu.VMEM((16, width), f32),
            pltpu.VMEM((18, tokens, width), bf16),
            pltpu.VMEM((width, 3 * cols), bf16),
            pltpu.VMEM((2, n_sp, N_Y, 16, width), bf16),
            pltpu.VMEM((18, tokens, cols), bf16),
            pltpu.VMEM((32 + 2 * n_sp, tokens, 2 * cols), bf16),
            pltpu.VMEM((16 * heads, 128), f32),
            pltpu.VMEM((16 * heads, GRID_W, 128), f32),
            pltpu.VMEM((4 * heads, 2 * GRID_W, KEY_ROWS * GRID_W), f32),
            pltpu.VMEM((4, samples, 2, tokens, cols), bf16),
            pltpu.VMEM((8, samples, tokens, cols), bf16),
            pltpu.VMEM((samples, tokens, width), bf16),
        ]
        + [dma(n) for n in sems],
        compiler_params=pltpu.CompilerParams(
            collective_id=1, has_side_effects=True, vmem_limit_bytes=60 * 2**20
        ),
    )(
        ctx_bias, cond, ctx_cond, w_shift, w_scale, w_gate, norm_gain[None, :], rel_bias.transpose(1, 0, 2),
        latent, context, w_query, w_key, w_value, w_out.reshape(n_sp, 16, width),
    )


def solution(mesh):
    return jax.shard_map(
        on_device,
        mesh=mesh,
        in_specs=(
            P(None, ("sp", "tp"), None),
            P(None, "sp", None),
            P(),
            P(),
            P("sp", "tp"),
            P("sp", "tp"),
            P("sp", "tp"),
            P(),
            P(None, "tp"),
            P(None, "tp"),
            P(None, "tp"),
            P("tp", None),
            P("tp", None, None),
            P("tp"),
        ),
        out_specs=P(None, ("sp", "tp"), None),
        check_vma=False,
    )
```

time: 95.2 us -> 74.5 us (0.78)
  Pallas kernels: 90.4 us -> 72.4 us
  local copies, waits for them, and re-layouts: 4.54 us -> 1.88 us
    pallas_call x1, Pallas kernels: 90.4 us -> 72.4 us  [on_device(): pl.pallas_call(block_kernel, out_shape=jax.ShapeDtypeStruct(latent.shape,...]
    unnamed x2 -> x1, local copies, waits for them, and re-layouts: 3.25 us -> 1.88 us
    broadcast_in_dim x1 -> x0, local copies, waits for them, and re-layouts: 1.28 us -> none  [on_device(): ctx_cond[None, :]]
where the time goes in v2:
time: 74.5 us; the launch traced here: 74.3 us
  Pallas kernels  72.4 us (97%)
  local copies, waits for them, and re-layouts  1.88 us (3%)
    pallas_call x1, Pallas kernels, on_device(): pl.pallas_call(block_kernel, out_shape=jax.ShapeDtypeStruct(latent.shape,...  72.4 us
    unnamed x1, local copies, waits for them, and re-layouts  1.88 us

profile of v2, /device:TPU:1, one launch (start us, length us, event | category | flops | bytes accessed | tf_op | source)
XLA Modules:
  0.0 74.3 jit_solution(1156992407227484409)
XLA Ops:
  0.0 72.4 %shard_map.136 = bf16[2,64,2048]{2,1,0:T(8,128)(2,1)} custom-call(f32[4]{0:T(128)} %far_ref.1, bf16[2,2048]{1,0:T(2,128)(2,1)} %cond_hbm.1, bf16[2048]{0:T(1024)(128)(2,1)} %cctx_hbm.1, bf16[128,256]{1,0:T(8,128)(2,1)} %ws_ref.1, bf16[128,256]{1,0:T(8,128)(2,1)} %wc_ref.1, bf16[128,256]{1,0:T(8,128)(2,1)} %wg_ref.1, f32[1,2048]{1,0:T(1,128)} %bitcast.5, ...), custom_call_target="tpu_custom_call" | custom-call | tf_op jit(solution)/shard_map/pallas_call | solution.py:494
  72.5 1.9 %copy.16 = bf16[2,64,2048]{2,1,0:T(8,128)(2,1)} copy(bf16[2,64,2048]{2,1,0:T(8,128)(2,1)} %shard_map.136) | data formatting | bytes 1048576

commit v3 on v2

v3 whole, which is shorter than its diff:
```python
import functools

import jax
import jax.numpy as jnp
from jax import lax
from jax.experimental import pallas as pl
from jax.experimental.pallas import tpu as pltpu
from jax.sharding import PartitionSpec as P

HEAD_DIM = 64
GRID_W = 64
WIN_ROWS = 8
WIN_COLS = 16
EPSILON = 1e-06
LOG2E = 1.4426950408889634
MESH = pl.DeviceIdType.MESH

N_X, N_Z, N_Y = 4, 4, 4
PAD_ROWS = 24
KEY_ROWS = 10
REACH = WIN_ROWS // 2


def remote(src, dst, send, recv, device):
    return pltpu.make_async_remote_copy(
        src_ref=src, dst_ref=dst, send_sem=send, recv_sem=recv, device_id=device, device_id_type=MESH
    )


class PlaneGather:
    HOPS = (0, 1, 1, 2)
    BACK = (0, 1, -1, 2)
    COUNTS = (4, 6, 4, 1)

    def __init__(self, block, x_first, place, way, tp, send, recv, landed=None):
        self.block, self.x_first, self.way, self.tp = block, x_first, way, tp
        self.z, self.x = place
        self.send, self.recv = send, recv
        self.landed = landed

    def at(self, first_back, second_back):
        step = lambda value, back: lax.rem(value + 8 - back * self.way, 4)
        if self.x_first:
            return step(self.z, second_back) * N_X + step(self.x, first_back)
        return step(self.z, first_back) * N_X + step(self.x, second_back)

    def pass_on(self, b, k, hops, first=0, second=0):
        ref = self.block(self.at(self.BACK[b], self.BACK[k]))
        remote(ref, ref, self.send, self.recv.at[hops - 1], (self.at(-first, -second), self.tp)).start()

    def have(self, b, k):
        hops = self.HOPS[b] + self.HOPS[k]
        if k == 0:
            if b == 0:
                self.pass_on(b, k, 1, first=1)
                self.pass_on(b, k, 1, first=-1)
            if b == 1:
                self.pass_on(b, k, 2, first=1)
            self.pass_on(b, k, hops + 1, second=1)
            self.pass_on(b, k, hops + 1, second=-1)
        if k == 1:
            self.pass_on(b, k, hops + 1, second=1)
        if self.landed:
            self.landed(self.at(self.BACK[b], self.BACK[k]))

    def start(self):
        self.have(0, 0)

    def round(self, r):
        for b, k in ((1, 0), (0, 1), (1, 1), (2, 0), (3, 0), (2, 1), (0, 2), (0, 3), (1, 2), (2, 2), (1, 3), (2, 3), (3, 1), (3, 2), (3, 3)):
            if self.HOPS[b] + self.HOPS[k] == r + 1:
                self.have(b, k)


class SampleGather(PlaneGather):
    def __init__(self, block, spare, xs, z, way, tp, send, recv):
        self.block, self.spare, self.xs, self.z, self.way, self.tp = block, spare, xs, z, way, tp
        self.send, self.recv = send, recv

    def z_at(self, back):
        return lax.rem(self.z + 8 - back * self.way, 4)

    def pass_on(self, b, k, hops, to_x=0, to_z=0):
        ref = self.block(N_X * self.z_at(self.BACK[k]) + self.xs[b])
        device = (N_X * self.z_at(-to_z) + self.xs[to_x], self.tp)
        remote(ref, ref, self.send, self.recv.at[hops - 1], device).start()

    def have(self, b, k):
        hops = self.HOPS[b] + self.HOPS[k]
        if k == 0:
            if b == 0:
                own = N_X * self.z + self.xs[0]
                partner = (N_X * self.z + self.xs[1], self.tp)
                remote(self.spare, self.block(own), self.send, self.recv.at[0], partner).start()
            if b < 2:
                self.pass_on(b, k, hops + 1, to_x=2)
            self.pass_on(b, k, hops + 1, to_z=1)
            self.pass_on(b, k, hops + 1, to_z=-1)
        if k == 1:
            self.pass_on(b, k, hops + 1, to_z=1)


def took(ref, sem):
    pltpu.make_async_copy(ref, ref, sem).wait()


def block_kernel(
    far_ref, cond_hbm, cctx_hbm, ws_ref, wc_ref, wg_ref, gain_hbm, bias_hbm, latent_ref, ctx_ref, wq_ref, wk_ref,
    wv_ref, wo_ref,
    out_ref,
    cond_ref, cctx_ref, w_mod, gain_ref, bias_ref, lat,
    ada, part, total_x, total, got_x, got_z, mod, buf, w, wo, q, kv, lines, diag, table, stage, att, out_buf,
    own_sem, sx, rx, sz, rz, sy, ry, s_ag, r_ag, s_sib, r_sib, s_halo, r_halo, s_ctx, r_ctx, s_w, r_w, r_wl,
    s_lat, r_lat, s_wy, r_wy, s_ws, r_ws, s_yr, r_yr, s_ys, r_ys, s_at, r_at, out_sem,
):
    sp, tp = lax.axis_index("sp"), lax.axis_index("tp")
    z, x = lax.div(sp, N_X), lax.rem(sp, N_X)
    y, c = lax.div(tp, 2), lax.rem(tp, 2)
    n_sp = N_X * N_Z
    way = 1 - 2 * c
    sib = 2 * y + 1 - c
    here = (sp, sib)
    cols = wq_ref.shape[1]
    share, late = 3 * buf.shape[2] // 8, buf.shape[2] // 4
    width = buf.shape[2]
    tokens = buf.shape[1]
    y_at = lambda back: lax.rem(y + 8 - back * way, 4)
    y_next = (sp, 2 * y_at(-1) + c)

    side, g = lax.rem(x, 2), lax.div(x, 2)
    smp = lax.rem(lax.div(x + 1, 2) + 1, 2)
    x_pair, x_across = x + 1 - 2 * side, 3 - x
    sp_pair = z * N_X + x_pair
    group = 2 * z + g
    up = lax.rem(z + g, N_Z) * N_X + x_across
    down = lax.rem(z + g + N_Z - 1, N_Z) * N_X + x_across
    beyond = lax.rem(z + 2 * g + N_Z - 1, N_Z) * N_X + x_across
    x_peers = [z * N_X + lax.rem(x + k, N_X) for k in range(1, N_X)]
    z_peers = [lax.rem(z + k, N_Z) * N_X + x for k in range(1, N_Z)]
    tp_peers = [lax.rem(tp + k, 8) for k in range(1, 8)]
    barrier = pltpu.get_barrier_semaphore()
    peers = [(p, tp) for p in x_peers + z_peers + [beyond]]
    peers += [(to, p) for p in tp_peers for to in (sp, sp_pair)]
    for device in peers:
        pl.semaphore_signal(barrier, inc=1, device_id=device, device_id_type=MESH)

    small = [
        pltpu.make_async_copy(src, dst, own_sem.at[8 + i])
        for i, (src, dst) in enumerate(
            ((cond_hbm, cond_ref), (cctx_hbm, cctx_ref), (ws_ref, w_mod.at[0]), (wc_ref, w_mod.at[1]), (wg_ref, w_mod.at[2]))
        )
    ]
    later = [pltpu.make_async_copy(gain_hbm, gain_ref, own_sem.at[13]), pltpu.make_async_copy(bias_hbm, bias_ref, own_sem.at[14])]
    own_lat = pltpu.make_async_copy(latent_ref, lat, own_sem.at[0])
    own_row = pltpu.make_async_copy(latent_ref.at[smp], buf.at[8 * side + tp], own_sem.at[1])
    own_wo = pltpu.make_async_copy(wo_ref, wo.at[c, :, 0], own_sem.at[2])
    own_ctx = [pltpu.make_async_copy(ctx_ref.at[s], buf.at[16 + s], own_sem.at[3 + s]) for s in range(2)]
    own_w = [
        pltpu.make_async_copy(ref, w.at[:, pl.ds(cols * i, cols)], own_sem.at[5 + i])
        for i, ref in enumerate((wq_ref, wk_ref, wv_ref))
    ]
    for copy in small + [own_wo, own_row, own_lat] + later + own_ctx + own_w:
        copy.start()

    ada[...] = jnp.zeros_like(ada)
    part[...] = jnp.zeros_like(part)
    kv[PAD_ROWS - 1] = jnp.zeros(kv.shape[1:], kv.dtype)
    columns = pl.ds(pl.multiple_of(sp * 128, 128), 128)
    for copy in small:
        copy.wait()
    ada[0:2, :] = cond_ref[:, columns].astype(jnp.float32)
    both = cctx_ref[pl.ds(pl.multiple_of(lax.div(sp, 2) * 256, 256), 256)].astype(jnp.float32).reshape(1, 256)
    ada[2:3, :] = jnp.where(lax.rem(sp, 2) == 0, both[:, :128], both[:, 128:])
    value = ada[...]
    value = (value / (1.0 + jnp.exp(-value))).astype(jnp.bfloat16)
    for i in range(3):
        rows = jnp.dot(value, w_mod[i], preferred_element_type=jnp.float32)
        part[3 * i : min(3 * i + 3, 8), :] = rows[: min(3, 8 - 3 * i)]
    pl.semaphore_wait(barrier, len(peers))

    for k, p in enumerate(x_peers):
        remote(part, got_x.at[k], sx.at[0], rx.at[0], (p, tp)).start()

    def row_at(slot, e):
        return 8 * lax.rem(side + e, 2) + slot

    def ag(k, e):
        ref = buf.at[row_at(2 * y_at(k) + c, e)]
        return remote(ref, ref, s_ag.at[0], r_ag.at[2 * k + e], y_next)

    def to_sib(j, e):
        ref = buf.at[row_at(2 * y_at(j) + c, e)]
        return remote(ref, ref, s_sib.at[0], r_sib.at[2 * j + e], here)

    to_pair = remote(lat.at[1 - smp], buf.at[8 * side + tp], s_lat.at[0], r_lat.at[0], (sp_pair, tp))

    def relay(k, s):
        ag(k, s).wait_recv()
        if k < 2:
            ag(k + 1, s).start()
        to_sib(k + 1, s).start()

    front, middle, back = pl.ds(0, share), pl.ds(share, late), pl.ds(share + late, width - share - late)
    early_late = pl.ds(0, share + late)

    def w_cross(d):
        return remote(
            wo.at[c, sp, 0, :, early_late], wo.at[c, sp, 4 - d, :, early_late], s_wy.at[0], r_wy.at[0],
            (sp, 2 * lax.rem(y + d, 4) + c),
        )

    def w_ring(k, h):
        ref = lambda at: wo.at[c, pl.ds(4 * h, 4), lax.rem(8 - at * way, 4), :, back]
        return remote(ref(k), ref(k + 1), s_yr.at[0], r_yr.at[4 * k + h], y_next)

    def w_ring_sib(k, h):
        ref = wo.at[c, pl.ds(4 * h, 4), lax.rem(8 - k * way, 4), :, back]
        return remote(ref, ref, s_ys.at[0], r_ys.at[0], here)

    def w_ring_round(k, h):
        w_ring(k, h).wait_recv()
        if k < 2:
            w_ring(k + 1, h).start()
        w_ring_sib(k + 1, h).start()

    def w_sib(rel, n, part, k):
        def landed(at):
            ref = wo.at[c, at, pl.ds(rel, n), :, part]
            remote(ref, ref, s_ws.at[k], r_ws.at[k], here).start()

        return landed

    own_wo.wait()
    for d in range(1, 4):
        w_cross(d).start()
    own_row.wait()
    ag(0, 0).start()
    own_lat.wait()
    to_pair.start()
    to_sib(0, 0).start()
    w_own = remote(wo.at[c, :, 0], wo.at[c, :, 0], s_ws.at[1], r_ws.at[1], here)
    w_own.start()
    for h in range(2):
        w_ring(0, h).start()

    ctx_gather = SampleGather(
        lambda at: kv.at[PAD_ROWS + at], kv.at[PAD_ROWS + n_sp], (x, x_pair, x_across, 3 - x_pair), z, way, tp,
        s_ctx.at[0], r_ctx,
    )
    def w_gathers(part, k, recv):
        return [
            PlaneGather(
                lambda at: wo.at[c, at, pl.ds(1, 2), :, part], False, (z, x), way, tp, s_w.at[k], recv, w_sib(1, 2, part, 2 * k)
            ),
            PlaneGather(
                lambda at: wo.at[c, at, pl.ds(3, 1), :, part], True, (z, x), way, tp, s_w.at[k], recv, w_sib(3, 1, part, 2 * k)
            ),
        ]

    w_early, w_late = w_gathers(front, 0, r_w), w_gathers(middle, 1, r_wl)

    def ctx_round(r):
        took(kv.at[pl.ds(0, PlaneGather.COUNTS[r])], r_ctx.at[r])
        ctx_gather.round(r)

    def w_round(r):
        took(wo.at[c, pl.ds(0, PlaneGather.COUNTS[r]), pl.ds(1, 3), :, front], r_w.at[r])
        for gather in w_early:
            gather.round(r)

    def w_late_round(r):
        took(wo.at[c, pl.ds(0, PlaneGather.COUNTS[r]), pl.ds(1, 3), :, middle], r_wl.at[r])
        for gather in w_late:
            gather.round(r)

    heads = bias_ref.shape[1]
    lines[...] = jnp.zeros_like(lines)
    for copy in later:
        copy.wait()
    for h in range(heads):
        lines[16 * h : 16 * h + 15, 0:31] = bias_ref[:, h, :]
    lines[...] = pltpu.roll(lines[...], 1, 0) + pltpu.roll(lines[...], GRID_W, 1)
    lane = lax.broadcasted_iota(jnp.int32, (GRID_W, 128), 1)
    col = lax.broadcasted_iota(jnp.int32, (GRID_W, 128), 0)
    first_col = jnp.clip(col - WIN_COLS // 2, 0, GRID_W - WIN_COLS)
    key_col = lax.rem(lane, GRID_W)
    col_ok = (key_col >= first_col) & (key_col < first_col + WIN_COLS)

    def tile(i, carry):
        line = jnp.broadcast_to(lines[pl.ds(i, 1), :], (GRID_W, 128))
        both = pltpu.roll(line, 128 - WIN_COLS + 1, 1, stride=1, stride_axis=0)
        diag[i] = jnp.where(col_ok, both * LOG2E, -jnp.inf)
        return carry

    took(got_x, sx.at[0])
    took(got_x, rx.at[0])
    total_x[...] = part[...] + got_x[0] + got_x[1] + got_x[2]
    for k, p in enumerate(z_peers):
        remote(total_x, got_z.at[k], sz.at[0], rz.at[0], (p, tp)).start()
    lax.fori_loop(0, 8 * heads, tile, 0, unroll=4)
    took(wo.at[c, 0, pl.ds(1, 3), :, early_late], r_wy.at[0])
    for gather in w_early:
        gather.start()
    took(got_z, sz.at[0])
    took(got_z, rz.at[0])
    value = total_x[...] + got_z[0] + got_z[1] + got_z[2]
    total[...] = value
    mine = pl.ds(pl.multiple_of(tp * cols, cols), cols)
    for k, p in enumerate(tp_peers):
        remote(total, mod.at[:, mine], sy.at[0], ry.at[0], (sp, p)).start()
    mod[:, mine] = value
    relay(0, 0)
    to_pair.wait_recv()
    ag(0, 1).start()
    to_sib(0, 1).start()
    lax.fori_loop(8 * heads, 16 * heads, tile, 0, unroll=4)
    w_round(0)
    for copy in own_ctx + own_w:
        copy.wait()
    took(mod.at[:, pl.ds(0, 7 * cols)], sy.at[0])
    took(mod.at[:, pl.ds(0, 7 * cols)], ry.at[0])

    factor = HEAD_DIM ** (-0.5) * LOG2E

    def halo(row, to, at):
        remote(kv.at[REACH + row], kv.at[at], s_halo.at[0], r_halo.at[0], (to, tp)).start()

    def step(i, carry):
        at = lax.max(i - 1, 0)
        rest = lax.max(at - 4, 0)
        last = lax.div(at, 4)
        j = last * (2 + lax.rem(rest, 2)) + (1 - last) * lax.div(at, 2)
        e = last * lax.div(rest, 2) + (1 - last) * lax.rem(at, 2)
        slot_a = 2 * y_at(j) + c
        slot_b = 2 * y_at(-j) + 1 - c
        latents = i > 0

        for at, k, half in ((1, 1, 0), (3, 0, 1), (5, 2, 0), (7, 1, 1), (8, 2, 1)):
            @pl.when(i == at)
            def _():
                relay(k, half)

        @pl.when(latents)
        def _():
            to_sib(j, e).wait_recv()

        zero = jnp.where(latents, 0, 1)
        at_a = zero * 16 + (1 - zero) * row_at(slot_a, e)
        at_b = zero * 17 + (1 - zero) * row_at(slot_b, e)
        which = zero * 2 + (1 - zero) * smp
        lift = gain_ref[...] * (1.0 + mod[pl.ds(3 + which, 1), :])
        shift = mod[pl.ds(which, 1), :]
        hidden = []
        for at in (at_a, at_b):
            rows = buf[at].astype(jnp.float32)
            inverse = lax.rsqrt(jnp.mean(rows * rows, axis=-1, keepdims=True) + EPSILON)
            hidden.append((rows * inverse * lift + shift).astype(jnp.bfloat16))
        got = jnp.dot(jnp.concatenate(hidden, axis=0), w[...], preferred_element_type=jnp.float32)
        query = (got[:, :cols] * factor).astype(jnp.bfloat16)
        pair = got[:, cols:].astype(jnp.bfloat16)
        q[at_a] = query[:tokens]
        q[at_b] = query[tokens:]
        mine_at, other_at = PAD_ROWS + sp, PAD_ROWS + n_sp
        kv_a = zero * (smp * other_at + (1 - smp) * mine_at) + (1 - zero) * (REACH + at_a)
        kv_b = zero * (smp * mine_at + (1 - smp) * other_at) + (1 - zero) * (REACH + at_b)
        kv[kv_a] = pair[:tokens]
        kv[kv_b] = pair[tokens:]

        for row in (at_a, at_b):
            @pl.when(latents & (row >= 12))
            def _():
                halo(row, up, row - 12)

            @pl.when(latents & (row <= 2))
            def _():
                halo(row, down, 20 + row)

        @pl.when(i == 0)
        def _():
            ctx_gather.start()

        @pl.when(i == 3)
        def _():
            ctx_round(0)
            w_round(1)

        @pl.when(i == 7)
        def _():
            w_ring_round(0, 0)
            w_ring_round(0, 1)
            for h in range(2, 4):
                w_ring(0, h).start()
            ctx_round(1)
            w_round(2)
            for gather in w_late:
                gather.start()

        @pl.when(i == 8)
        def _():
            w_round(3)

        return carry

    lax.fori_loop(0, 9, step, 0)

    def fill(i, carry):
        k, h = lax.div(i, heads), lax.rem(i, heads)
        p = k + 3 * lax.div(k, 3)
        g0 = 16 * group + 2 * p
        start = jnp.clip(g0 - REACH, 0, 8 * n_sp - KEY_ROWS)
        for a in range(2):
            r0 = jnp.clip(g0 + a - REACH, 0, 8 * n_sp - WIN_ROWS)
            for v in range(0, KEY_ROWS, 2):
                e = jnp.clip(start - g0 - a + WIN_ROWS + v, 0, 15)
                row = start + v + lax.div(lane, GRID_W)
                ok = (row >= r0) & (row < r0 + WIN_ROWS)
                table[i, GRID_W * a : GRID_W * (a + 1), GRID_W * v : GRID_W * (v + 2)] = jnp.where(
                    ok, diag[16 * h + e], -jnp.inf
                )
        return carry

    w_ring_round(1, 0)
    w_ring_round(1, 1)
    ctx_round(2)
    lax.fori_loop(0, 5 * heads, fill, 0)
    w_ring_round(0, 2)
    w_ring_round(0, 3)
    took(kv.at[pl.ds(0, 7)], r_halo.at[0])
    ctx_round(3)
    w_late_round(0)

    contract = (((1,), (1,)), ((), ()))
    nq = 2 * GRID_W
    low = lax.broadcasted_iota(jnp.int32, (nq, 128), 1) < HEAD_DIM
    first_head = lax.broadcasted_iota(jnp.int32, (2 * nq, 1), 0) < nq

    def pair_at(idx):
        return 4 * lax.rem(side + 1 + lax.div(idx, 4), 2) + lax.rem(y + 1 + idx, 4)

    def attended_to(idx, there):
        own = lax.div(idx, 4)
        device = (own * sp + (1 - own) * sp_pair, 2 * lax.rem(y + 1 + idx, 4) + there)
        return remote(stage.at[idx, there], att.at[tp, smp], s_at.at[0], r_at.at[0], device)

    ones = lambda values: jnp.concatenate([values, jnp.ones_like(values)], axis=1)

    def attend(it, carry):
        context = pl.ds(PAD_ROWS, n_sp)
        for u in range(1):
            idx = it + u
            p = pair_at(idx)
            start = jnp.clip(16 * group + 2 * p - REACH, 0, 8 * n_sp - KEY_ROWS) - (16 * group - REACH)
            rows = pl.ds(start, KEY_ROWS)
            kind = lax.min(p, 2) + lax.max(p - 5, 0)
            outs = []
            for lp in range(2):
                keys, values = slice(128 * lp, 128 * lp + 128), slice(cols + 128 * lp, cols + 128 * lp + 128)
                one = q[pl.ds(2 * p, 2), :, keys].reshape(nq, 128)
                none = jnp.zeros_like(one)
                both = jnp.concatenate([jnp.where(low, one, none), jnp.where(low, none, one)], axis=0)
                near = lax.dot_general(
                    both, kv[rows, :, keys].reshape(-1, 128), contract, preferred_element_type=jnp.float32
                )
                near = near + table[pl.ds(heads * kind + 2 * lp, 2)].reshape(2 * nq, -1)
                far = lax.dot_general(
                    both, kv[context, :, keys].reshape(-1, 128), contract, preferred_element_type=jnp.float32
                )
                lift = jnp.where(first_head, far_ref[2 * lp], far_ref[2 * lp + 1]) * LOG2E
                top = jnp.maximum(jnp.max(near, axis=-1, keepdims=True), jnp.max(far, axis=-1, keepdims=True) + lift)
                near = jnp.exp2(near - top).astype(jnp.bfloat16)
                far = jnp.exp2(far - (top - lift)).astype(jnp.bfloat16)
                got = jnp.dot(near, ones(kv[rows, :, values].reshape(-1, 128)), preferred_element_type=jnp.float32)
                got = got + jnp.dot(
                    far, ones(kv[context, :, values].reshape(-1, 128)), preferred_element_type=jnp.float32
                )
                got = got[:, :128] / got[:, 128:]
                outs.append(jnp.where(low, got[:nq], got[nq:]).astype(jnp.bfloat16))
            done = jnp.concatenate(outs, axis=1)
            stage[idx, 0] = done[:GRID_W]
            stage[idx, 1] = done[GRID_W:]

        @pl.when(it < 7)
        def _():
            attended_to(it, 0).start()
            attended_to(it, 1).start()

        @pl.when(it == 7)
        def _():
            attended_to(7, 1 - c).start()
            att[tp, smp] = stage[7, c]

        for at, todo in ((0, ((1, 2),)), (1, ((1, 3), (2, 0))), (2, ((2, 1),)), (3, ((2, 2),)), (4, ((2, 3),))):
            @pl.when(it == at)
            def _():
                for k, h in todo:
                    w_ring_round(k, h)

        for at, r in ((2, 1), (5, 2), (7, 3)):
            @pl.when(it == at)
            def _():
                w_late_round(r)

        return carry

    lax.fori_loop(0, 8, attend, 0)

    took(wo.at[1 - c, :, pl.ds(1, 3), :, front], r_ws.at[0])
    took(wo.at[1 - c, :, pl.ds(1, 3), :, middle], r_ws.at[2])
    took(wo.at[1 - c, :, 0], r_ws.at[1])
    took(wo.at[1 - c, :, pl.ds(1, 3), :, back], r_ys.at[0])
    took(q.at[pl.ds(0, 15)], r_at.at[0])

    def project(n, carry):
        at = pl.ds(pl.multiple_of(512 * n, 512), 512)
        acc = jnp.zeros((2 * tokens, 512), jnp.float32)
        for core in range(2):
            for rel in range(4):
                rows = att[2 * lax.rem(y + rel, 4) + core].reshape(2 * tokens, cols)
                weight = wo[core, :, rel, :, at].reshape(cols, 512)
                acc = acc + jnp.dot(rows, weight, preferred_element_type=jnp.float32)
        for s in range(2):
            mixed = lat[s, :, at].astype(jnp.float32) + mod[6 + s : 7 + s, at] * acc[s * tokens : (s + 1) * tokens]
            out_buf[s, :, at] = mixed.astype(jnp.bfloat16)
        pltpu.make_async_copy(out_buf.at[:, :, at], out_ref.at[:, :, at], out_sem.at[n]).start()
        return carry

    lax.fori_loop(0, width // 512, project, 0)

    took(buf.at[pl.ds(0, 6)], s_ag.at[0])
    took(buf.at[pl.ds(0, 8)], s_sib.at[0])
    took(kv.at[pl.ds(0, 7)], s_halo.at[0])
    took(kv.at[pl.ds(0, 15)], s_ctx.at[0])
    to_pair.wait_send()
    took(wo.at[c, pl.ds(0, 15), pl.ds(1, 3), :, front], s_w.at[0])
    took(wo.at[c, pl.ds(0, 15), pl.ds(1, 3), :, middle], s_w.at[1])
    took(wo.at[c, 0, pl.ds(1, 3), :, early_late], s_wy.at[0])
    took(wo.at[c, :, pl.ds(1, 3), :, front], s_ws.at[0])
    took(wo.at[c, :, pl.ds(1, 3), :, middle], s_ws.at[2])
    took(wo.at[c, :, 0], s_ws.at[1])
    took(wo.at[c, :, pl.ds(1, 3), :, back], s_yr.at[0])
    took(wo.at[c, :, pl.ds(1, 3), :, back], s_ys.at[0])
    took(q.at[pl.ds(0, 15)], s_at.at[0])
    for n in range(width // 512):
        at = pl.ds(512 * n, 512)
        pltpu.make_async_copy(out_buf.at[:, :, at], out_ref.at[:, :, at], out_sem.at[n]).wait()


def on_device(
    latent, context, cond, ctx_cond, w_shift, w_scale, w_gate, norm_gain,
    w_query, w_key, w_value, w_out, rel_bias, ctx_bias,
):
    samples, tokens, width = latent.shape
    cols = w_query.shape[1]
    heads = cols // HEAD_DIM
    n_sp = N_X * N_Z
    anywhere = pl.BlockSpec(memory_space=pl.ANY)
    f32, bf16 = jnp.float32, jnp.bfloat16
    dma = lambda n: pltpu.SemaphoreType.DMA((n,))
    sems = [15, 1, 1, 1, 1, 1, 1, 1, 6, 1, 8, 1, 1, 1, 4, 2, 4, 4]
    sems += [1, 1, 1, 1, 3, 3, 1, 12, 1, 1, 1, 1, 4]
    return pl.pallas_call(
        block_kernel,
        out_shape=jax.ShapeDtypeStruct(latent.shape, bf16),
        in_specs=[pl.BlockSpec(memory_space=pltpu.SMEM)] + [anywhere] * 13,
        out_specs=anywhere,
        scratch_shapes=[
            pltpu.VMEM(cond.shape, bf16),
            pltpu.VMEM(ctx_cond.shape, bf16),
            pltpu.VMEM((3,) + w_shift.shape, bf16),
            pltpu.VMEM((1, width), f32),
            pltpu.VMEM((15, heads, 31), f32),
            pltpu.VMEM(latent.shape, bf16),
            pltpu.VMEM((8, 128), f32),
            pltpu.VMEM((8, cols), f32),
            pltpu.VMEM((8, cols), f32),
            pltpu.VMEM((8, cols), f32),
            pltpu.VMEM((3, 8, cols), f32),
            pltpu.VMEM((3, 8, cols), f32),
            pltpu.VMEM((8, width), f32),
            pltpu.VMEM((18, tokens, width), bf16),
            pltpu.VMEM((width, 3 * cols), bf16),
            pltpu.VMEM((2, n_sp, N_Y, 16, width), bf16),
            pltpu.VMEM((18, tokens, cols), bf16),
            pltpu.VMEM((PAD_ROWS + n_sp + 1, tokens, 2 * cols), bf16),
            pltpu.VMEM((16 * heads, 128), f32),
            pltpu.VMEM((16 * heads, GRID_W, 128), f32),
            pltpu.VMEM((5 * heads, 2 * GRID_W, KEY_ROWS * GRID_W), f32),
            pltpu.VMEM((8, 2, tokens, cols), bf16),
            pltpu.VMEM((8, samples, tokens, cols), bf16),
            pltpu.VMEM((samples, tokens, width), bf16),
        ]
        + [dma(n) for n in sems],
        compiler_params=pltpu.CompilerParams(
            collective_id=1, has_side_effects=True, vmem_limit_bytes=60 * 2**20
        ),
    )(
        ctx_bias, cond, ctx_cond, w_shift, w_scale, w_gate, norm_gain[None, :], rel_bias.transpose(1, 0, 2),
        latent, context, w_query, w_key, w_value, w_out.reshape(n_sp, 16, width),
    )


def solution(mesh):
    return jax.shard_map(
        on_device,
        mesh=mesh,
        in_specs=(
            P(None, ("sp", "tp"), None),
            P(None, "sp", None),
            P(),
            P(),
            P("sp", "tp"),
            P("sp", "tp"),
            P("sp", "tp"),
            P(),
            P(None, "tp"),
            P(None, "tp"),
            P(None, "tp"),
            P("tp", None),
            P("tp", None, None),
            P("tp"),
        ),
        out_specs=P(None, ("sp", "tp"), None),
        check_vma=False,
    )
```

time: 74.5 us -> 66.2 us (0.89)
  Pallas kernels: 72.4 us -> 64.2 us
    pallas_call x1, Pallas kernels: 72.4 us -> 64.2 us  [on_device(): pl.pallas_call(block_kernel, out_shape=jax.ShapeDtypeStruct(latent.shape,...]
where the time goes in v3:
time: 66.2 us; the launch traced here: 66.1 us
  Pallas kernels  64.2 us (97%)
  local copies, waits for them, and re-layouts  1.88 us (3%)
    pallas_call x1, Pallas kernels, on_device(): pl.pallas_call(block_kernel, out_shape=jax.ShapeDtypeStruct(latent.shape,...  64.2 us
    unnamed x1, local copies, waits for them, and re-layouts  1.88 us

profile of v3, /device:TPU:1, one launch (start us, length us, event | category | flops | bytes accessed | tf_op | source)
XLA Modules:
  0.0 66.1 jit_solution(6461790659832039709)
XLA Ops:
  0.0 64.2 %shard_map.136 = bf16[2,64,2048]{2,1,0:T(8,128)(2,1)} custom-call(f32[4]{0:T(128)} %far_ref.1, bf16[2,2048]{1,0:T(2,128)(2,1)} %cond_hbm.1, bf16[2048]{0:T(1024)(128)(2,1)} %cctx_hbm.1, bf16[128,256]{1,0:T(8,128)(2,1)} %ws_ref.1, bf16[128,256]{1,0:T(8,128)(2,1)} %wc_ref.1, bf16[128,256]{1,0:T(8,128)(2,1)} %wg_ref.1, f32[1,2048]{1,0:T(1,128)} %bitcast.5, ...), custom_call_target="tpu_custom_call" | custom-call | tf_op jit(solution)/shard_map/pallas_call | solution.py:561
  64.2 1.9 %copy.16 = bf16[2,64,2048]{2,1,0:T(8,128)(2,1)} copy(bf16[2,64,2048]{2,1,0:T(8,128)(2,1)} %shard_map.136) | data formatting | bytes 1048576

commit v4 on v3

--- a/solution.py
+++ b/solution.py
@@ -314,6 +314,23 @@
     ag(0, 1).start()
     to_sib(0, 1).start()
     lax.fori_loop(8 * heads, 16 * heads, tile, 0, unroll=4)
+    def fill(i, carry):
+        k, h = lax.div(i, heads), lax.rem(i, heads)
+        p = k + 3 * lax.div(k, 3)
+        g0 = 16 * group + 2 * p
+        start = jnp.clip(g0 - REACH, 0, 8 * n_sp - KEY_ROWS)
+        for a in range(2):
+            r0 = jnp.clip(g0 + a - REACH, 0, 8 * n_sp - WIN_ROWS)
+            for v in range(0, KEY_ROWS, 2):
+                e = jnp.clip(start - g0 - a + WIN_ROWS + v, 0, 15)
+                row = start + v + lax.div(lane, GRID_W)
+                ok = (row >= r0) & (row < r0 + WIN_ROWS)
+                table[i, GRID_W * a : GRID_W * (a + 1), GRID_W * v : GRID_W * (v + 2)] = jnp.where(
+                    ok, diag[16 * h + e], -jnp.inf
+                )
+        return carry
+
+    lax.fori_loop(0, 5 * heads, fill, 0)
     w_round(0)
     for copy in own_ctx + own_w:
         copy.wait()
@@ -339,6 +356,14 @@
             @pl.when(i == at)
             def _():
                 relay(k, half)
+
+        @pl.when(i == 7)
+        def _():
+            ctx_round(1)
+
+        @pl.when(i == 8)
+        def _():
+            ctx_round(2)
 
         @pl.when(latents)
         def _():
@@ -390,7 +415,6 @@
             w_ring_round(0, 1)
             for h in range(2, 4):
                 w_ring(0, h).start()
-            ctx_round(1)
             w_round(2)
             for gather in w_late:
                 gather.start()
@@ -403,29 +427,10 @@
 
     lax.fori_loop(0, 9, step, 0)
 
-    def fill(i, carry):
-        k, h = lax.div(i, heads), lax.rem(i, heads)
-        p = k + 3 * lax.div(k, 3)
-        g0 = 16 * group + 2 * p
-        start = jnp.clip(g0 - REACH, 0, 8 * n_sp - KEY_ROWS)
-        for a in range(2):
-            r0 = jnp.clip(g0 + a - REACH, 0, 8 * n_sp - WIN_ROWS)
-            for v in range(0, KEY_ROWS, 2):
-                e = jnp.clip(start - g0 - a + WIN_ROWS + v, 0, 15)
-                row = start + v + lax.div(lane, GRID_W)
-                ok = (row >= r0) & (row < r0 + WIN_ROWS)
-                table[i, GRID_W * a : GRID_W * (a + 1), GRID_W * v : GRID_W * (v + 2)] = jnp.where(
-                    ok, diag[16 * h + e], -jnp.inf
-                )
-        return carry
-
     w_ring_round(1, 0)
     w_ring_round(1, 1)
-    ctx_round(2)
-    lax.fori_loop(0, 5 * heads, fill, 0)
     w_ring_round(0, 2)
     w_ring_round(0, 3)
-    took(kv.at[pl.ds(0, 7)], r_halo.at[0])
     ctx_round(3)
     w_late_round(0)
 
@@ -435,16 +440,23 @@
     first_head = lax.broadcasted_iota(jnp.int32, (2 * nq, 1), 0) < nq
 
     def pair_at(idx):
-        return 4 * lax.rem(side + 1 + lax.div(idx, 4), 2) + lax.rem(y + 1 + idx, 4)
+        outer = lax.div(idx, 4)
+        return (1 - outer) * (2 + lax.rem(idx, 4)) + outer * lax.rem(6 + lax.rem(y + 3 + idx, 4), 8)
 
     def attended_to(idx, there):
-        own = lax.div(idx, 4)
-        device = (own * sp + (1 - own) * sp_pair, 2 * lax.rem(y + 1 + idx, 4) + there)
-        return remote(stage.at[idx, there], att.at[tp, smp], s_at.at[0], r_at.at[0], device)
+        p = pair_at(idx)
+        to = z * N_X + 2 * g + lax.div(p, 4)
+        return remote(
+            stage.at[idx, there], att.at[tp, smp], s_at.at[0], r_at.at[0], (to, 2 * lax.rem(p, 4) + there)
+        )
 
     ones = lambda values: jnp.concatenate([values, jnp.ones_like(values)], axis=1)
 
     def attend(it, carry):
+        @pl.when(it == 4)
+        def _():
+            took(kv.at[pl.ds(0, 7)], r_halo.at[0])
+
         context = pl.ds(PAD_ROWS, n_sp)
         for u in range(1):
             idx = it + u
@@ -479,23 +491,24 @@
             stage[idx, 0] = done[:GRID_W]
             stage[idx, 1] = done[GRID_W:]
 
-        @pl.when(it < 7)
-        def _():
-            attended_to(it, 0).start()
-            attended_to(it, 1).start()
-
-        @pl.when(it == 7)
-        def _():
-            attended_to(7, 1 - c).start()
-            att[tp, smp] = stage[7, c]
-
-        for at, todo in ((0, ((1, 2),)), (1, ((1, 3), (2, 0))), (2, ((2, 1),)), (3, ((2, 2),)), (4, ((2, 3),))):
+        for there in range(2):
+            here_too = (pair_at(it) == 4 * side + y) & (c == there)
+
+            @pl.when(jnp.logical_not(here_too))
+            def _():
+                attended_to(it, there).start()
+
+            @pl.when(here_too)
+            def _():
+                att[tp, smp] = stage[it, there]
+
+        for at, todo in ((1, ((2, 0),)), (2, ((1, 2),)), (3, ((1, 3),)), (4, ((2, 1),)), (5, ((2, 2),)), (6, ((2, 3),))):
             @pl.when(it == at)
             def _():
                 for k, h in todo:
                     w_ring_round(k, h)
 
-        for at, r in ((2, 1), (5, 2), (7, 3)):
+        for at, r in ((3, 1), (5, 2), (7, 3)):
             @pl.when(it == at)
             def _():
                 w_late_round(r)

time: 66.2 us -> 65.8 us (level)
  no operation moved by 1% of the time
where the time goes in v4:
time: 65.8 us; the launch traced here: 65.6 us
  Pallas kernels  63.8 us (97%)
  local copies, waits for them, and re-layouts  1.88 us (3%)
    pallas_call x1, Pallas kernels, on_device(): pl.pallas_call(block_kernel, out_shape=jax.ShapeDtypeStruct(latent.shape,...  63.8 us
    unnamed x1, local copies, waits for them, and re-layouts  1.88 us

profile of v4, /device:TPU:1, one launch (start us, length us, event | category | flops | bytes accessed | tf_op | source)
XLA Modules:
  0.0 65.6 jit_solution(14401771443367266994)
XLA Ops:
  0.0 63.8 %shard_map.136 = bf16[2,64,2048]{2,1,0:T(8,128)(2,1)} custom-call(f32[4]{0:T(128)} %far_ref.1, bf16[2,2048]{1,0:T(2,128)(2,1)} %cond_hbm.1, bf16[2048]{0:T(1024)(128)(2,1)} %cctx_hbm.1, bf16[128,256]{1,0:T(8,128)(2,1)} %ws_ref.1, bf16[128,256]{1,0:T(8,128)(2,1)} %wc_ref.1, bf16[128,256]{1,0:T(8,128)(2,1)} %wg_ref.1, f32[1,2048]{1,0:T(1,128)} %bitcast.5, ...), custom_call_target="tpu_custom_call" | custom-call | tf_op jit(solution)/shard_map/pallas_call | solution.py:574
  63.8 1.9 %copy.16 = bf16[2,64,2048]{2,1,0:T(8,128)(2,1)} copy(bf16[2,64,2048]{2,1,0:T(8,128)(2,1)} %shard_map.136) | data formatting | bytes 1048576

commit v5 on v4

--- a/solution.py
+++ b/solution.py
@@ -453,13 +453,13 @@
     ones = lambda values: jnp.concatenate([values, jnp.ones_like(values)], axis=1)
 
     def attend(it, carry):
-        @pl.when(it == 4)
+        @pl.when(it == 2)
         def _():
             took(kv.at[pl.ds(0, 7)], r_halo.at[0])
 
         context = pl.ds(PAD_ROWS, n_sp)
-        for u in range(1):
-            idx = it + u
+        for u in range(2):
+            idx = 2 * it + u
             p = pair_at(idx)
             start = jnp.clip(16 * group + 2 * p - REACH, 0, 8 * n_sp - KEY_ROWS) - (16 * group - REACH)
             rows = pl.ds(start, KEY_ROWS)
@@ -491,31 +491,32 @@
             stage[idx, 0] = done[:GRID_W]
             stage[idx, 1] = done[GRID_W:]
 
-        for there in range(2):
-            here_too = (pair_at(it) == 4 * side + y) & (c == there)
+        for u, there in ((0, 0), (0, 1), (1, 0), (1, 1)):
+            idx = 2 * it + u
+            here_too = (pair_at(idx) == 4 * side + y) & (c == there)
 
             @pl.when(jnp.logical_not(here_too))
             def _():
-                attended_to(it, there).start()
+                attended_to(idx, there).start()
 
             @pl.when(here_too)
             def _():
-                att[tp, smp] = stage[it, there]
-
-        for at, todo in ((1, ((2, 0),)), (2, ((1, 2),)), (3, ((1, 3),)), (4, ((2, 1),)), (5, ((2, 2),)), (6, ((2, 3),))):
+                att[tp, smp] = stage[idx, there]
+
+        for at, todo in ((0, ((2, 0),)), (1, ((1, 2), (1, 3))), (2, ((2, 1), (2, 2))), (3, ((2, 3),))):
             @pl.when(it == at)
             def _():
                 for k, h in todo:
                     w_ring_round(k, h)
 
-        for at, r in ((3, 1), (5, 2), (7, 3)):
+        for at, r in ((1, 1), (2, 2), (3, 3)):
             @pl.when(it == at)
             def _():
                 w_late_round(r)
 
         return carry
 
-    lax.fori_loop(0, 8, attend, 0)
+    lax.fori_loop(0, 4, attend, 0)
 
     took(wo.at[1 - c, :, pl.ds(1, 3), :, front], r_ws.at[0])
     took(wo.at[1 - c, :, pl.ds(1, 3), :, middle], r_ws.at[2])

time: 65.8 us -> 66.6 us (1.012)
  no operation moved by 1% of the time
where the time goes in v5:
time: 66.6 us; the launch traced here: 66.1 us
  Pallas kernels  64.2 us (96%)
  local copies, waits for them, and re-layouts  1.88 us (3%)
    pallas_call x1, Pallas kernels, on_device(): pl.pallas_call(block_kernel, out_shape=jax.ShapeDtypeStruct(latent.shape,...  64.2 us
    unnamed x1, local copies, waits for them, and re-layouts  1.88 us

profile of v5, /device:TPU:1, one launch (start us, length us, event | category | flops | bytes accessed | tf_op | source)
XLA Modules:
  0.0 66.1 jit_solution(4931423841446638288)
XLA Ops:
  0.0 64.2 %shard_map.136 = bf16[2,64,2048]{2,1,0:T(8,128)(2,1)} custom-call(f32[4]{0:T(128)} %far_ref.1, bf16[2,2048]{1,0:T(2,128)(2,1)} %cond_hbm.1, bf16[2048]{0:T(1024)(128)(2,1)} %cctx_hbm.1, bf16[128,256]{1,0:T(8,128)(2,1)} %ws_ref.1, bf16[128,256]{1,0:T(8,128)(2,1)} %wc_ref.1, bf16[128,256]{1,0:T(8,128)(2,1)} %wg_ref.1, f32[1,2048]{1,0:T(1,128)} %bitcast.5, ...), custom_call_target="tpu_custom_call" | custom-call | tf_op jit(solution)/shard_map/pallas_call | solution.py:575
  64.2 1.9 %copy.16 = bf16[2,64,2048]{2,1,0:T(8,128)(2,1)} copy(bf16[2,64,2048]{2,1,0:T(8,128)(2,1)} %shard_map.136) | data formatting | bytes 1048576
